TPU v7x, 128 devices: a whole 4x4x4 slice. The times are simulated.
128 devices in a mesh: ep: 64 (over z, y, x), tp: 2 (over core).
Axes of the slice: x: 4, y: 4, z: 4, core: 2. Of those that a mesh axis runs over, the one named last changes fastest.
Arguments:
- hidden: bfloat16 [4096, 2048], P('ep'), may hold values from -6 to 6
- mix_gain: float32 [2048], replicated, may hold values from 0.1 to 1.9
- recept_weight: bfloat16 [2048, 1024], P(None, 'tp'), may hold values from -0.125 to 0.125
- key_weight: bfloat16 [2048, 1024], P(None, 'tp'), may hold values from -0.125 to 0.125
- value_weight: bfloat16 [2048, 1024], P(None, 'tp'), may hold values from -0.125 to 0.125
- decay_down: bfloat16 [2048, 64], replicated, may hold values from -0.125 to 0.125
- decay_up: bfloat16 [64, 1024], replicated, may hold values from -0.75 to 0.75
- decay_bias: float32 [1024], replicated, may hold values from -4 to 1
- rate_down: bfloat16 [2048, 64], replicated, may hold values from -0.125 to 0.125
- rate_up: bfloat16 [64, 1024], replicated, may hold values from -0.75 to 0.75
- rate_bias: float32 [1024], replicated, may hold values from -4 to 4
- head_gain: float32 [1024], replicated, may hold values from 0.1 to 1.9
- out_weight: bfloat16 [1024, 2048], P('tp'), may hold values from -0.1875 to 0.1875
- memory_state: float32 [4096, 16, 64, 64], P('ep', 'tp'), may hold values from -6 to 6
- ffn_gain: float32 [2048], replicated, may hold values from 0.1 to 1.9
- blend_vector: bfloat16 [2048], replicated, may hold values from -0.125 to 0.125
- dense_gate: bfloat16 [2048, 5632], P(None, ('ep', 'tp')), may hold values from -0.125 to 0.125
- dense_up: bfloat16 [2048, 5632], P(None, ('ep', 'tp')), may hold values from -0.125 to 0.125
- dense_down: bfloat16 [5632, 2048], P(('ep', 'tp')), may hold values from -0.3125 to 0.3125
- expert_gate: bfloat16 [64, 2048, 1536], P('ep', None, 'tp'), may hold values from -0.125 to 0.125
- expert_up: bfloat16 [64, 2048, 1536], P('ep', None, 'tp'), may hold values from -0.125 to 0.125
- expert_down: bfloat16 [64, 1536, 2048], P('ep', 'tp'), may hold values from -0.15625 to 0.15625
- routing: int32 [4096, 2], P('ep'), may hold values from 0 to 63, all different within a row; in each aligned block of 64 rows (0 to 63, 64 to 127, ...) at most 4 rows name the same one
- route_scale: float32 [4096, 2], P('ep'), may hold values from 0.25 to 1
Outputs:
- layer_out: bfloat16 [4096, 2048], P('ep')
- new_state: float32 [4096, 16, 64, 64], P('ep', 'tp')
Inputs may be any that keep to these rules, and one draw needn't show every extreme that they name: `routing`: among the 64 sequences of one index of ep, no expert is chosen more than 4 times, and some expert is chosen exactly 4 times; a sequence's 2 choices differ.
All inputs are finite; a program needn't handle non-finite values.
Results may differ from a plain program's by a relative error of at most 0.017.
Values may be sent and summed in bfloat16 or wider, within the bound.
A program may use at most 192 MiB of HBM per device.

v0:
```python
import jax
import jax.numpy as jnp
from jax import lax
from jax.sharding import PartitionSpec as P


def copy_for_each(x, axis):
    length = lax.axis_size(axis)
    return lax.all_to_all(jnp.broadcast_to(x[None], (length, *x.shape)), axis, 0, 0, tiled=True)


def of_everyone(x, axis):
    everything = copy_for_each(x, axis)
    return jnp.sum(everything.astype(jnp.float32), axis=0)


def stored(tensor):
    return lax.optimization_barrier(tensor.astype(jnp.bfloat16)).astype(jnp.float32)


def rms_scaled(tensor, gain_vec):
    values = tensor.astype(jnp.float32)
    return values * lax.rsqrt(jnp.mean(values * values, axis=-1, keepdims=True) + 1e-06) * gain_vec


def silu_of(tensor):
    return tensor / (1.0 + jnp.exp(-tensor))


def matmul(left, right):
    return jnp.dot(left, right, preferred_element_type=jnp.float32)


def shards(
    hidden,
    mix_gain,
    recept_weight,
    key_weight,
    value_weight,
    decay_down,
    decay_up,
    decay_bias,
    rate_down,
    rate_up,
    rate_bias,
    head_gain,
    out_weight,
    memory_state,
    ffn_gain,
    blend_vector,
    dense_gate,
    dense_up,
    dense_down,
    expert_gate,
    expert_up,
    expert_down,
    routing,
    route_scale,
):
    seq_count, model_width = hidden.shape
    own_width = recept_weight.shape[1]
    head_count = memory_state.shape[1]
    head_size = memory_state.shape[2]
    offset = lax.axis_index("tp") * own_width
    decay_up_own = lax.dynamic_slice_in_dim(decay_up, offset, own_width, 1)
    rate_up_own = lax.dynamic_slice_in_dim(rate_up, offset, own_width, 1)
    decay_bias_own = lax.dynamic_slice_in_dim(decay_bias, offset, own_width, 0)
    rate_bias_own = lax.dynamic_slice_in_dim(rate_bias, offset, own_width, 0)
    gain_own = lax.dynamic_slice_in_dim(head_gain, offset, own_width, 0)
    normed_in = rms_scaled(hidden, mix_gain).astype(jnp.bfloat16)
    split_shape = (seq_count, head_count, head_size)
    recept_rows = stored(matmul(normed_in, recept_weight)).reshape(split_shape)
    key_rows = stored(matmul(normed_in, key_weight)).reshape(split_shape)
    value_rows = stored(matmul(normed_in, value_weight)).reshape(split_shape)
    decay_low = jnp.tanh(matmul(normed_in, decay_down)).astype(jnp.bfloat16)
    decay_pre = matmul(decay_low, decay_up_own) + decay_bias_own
    decay_rate = jnp.exp(-jnp.exp(-jax.nn.softplus(-decay_pre) - 0.5)).reshape(split_shape)
    rate_low = matmul(normed_in, rate_down).astype(jnp.bfloat16)
    learn_rate = jax.nn.sigmoid(matmul(rate_low, rate_up_own) + rate_bias_own).reshape(split_shape)
    unit_key = key_rows * lax.rsqrt(jnp.sum(key_rows * key_rows, axis=-1, keepdims=True) + 1e-06)
    removed = jnp.einsum("shij,shj->shi", memory_state, unit_key)
    new_state = (
        memory_state * decay_rate[:, :, None, :]
        - removed[..., None] * (unit_key * learn_rate)[:, :, None, :]
        + value_rows[..., None] * (key_rows * learn_rate)[:, :, None, :]
    )
    readout = jnp.einsum("shij,shj->shi", new_state, recept_rows)
    centre = jnp.mean(readout, axis=-1, keepdims=True)
    variance = jnp.mean(jnp.square(readout - centre), axis=-1, keepdims=True)
    head_normed = (
        (
            (readout - centre)
            * lax.rsqrt(variance + 0.00064)
            * gain_own.reshape(head_count, head_size)
        )
        .astype(jnp.bfloat16)
        .reshape(seq_count, own_width)
    )
    attn_sum = of_everyone(matmul(head_normed, out_weight).astype(jnp.bfloat16), "tp").astype(
        jnp.float32
    )
    first_res = (hidden.astype(jnp.float32) + attn_sum).astype(jnp.bfloat16)
    ffn_in = rms_scaled(first_res, ffn_gain).astype(jnp.bfloat16)
    blend = jax.nn.sigmoid(jnp.dot(ffn_in, blend_vector, preferred_element_type=jnp.float32))
    piece = lax.all_gather(ffn_in, "ep", axis=0, tiled=True)
    dense_act = (silu_of(matmul(piece, dense_gate)) * matmul(piece, dense_up)).astype(jnp.bfloat16)
    own_units = lax.all_to_all(dense_act, "ep", split_axis=0, concat_axis=1, tiled=True)
    dense_out = matmul(own_units, lax.all_gather(dense_down, "ep", axis=0, tiled=True))
    dest_count = lax.axis_size("ep")
    top_count = routing.shape[1]
    slot_cap = max(2, 2 * seq_count * top_count // dest_count)
    flat_route = routing.reshape(-1)
    one_hot = (flat_route[:, None] == jnp.arange(dest_count, dtype=jnp.int32)[None, :]).astype(
        jnp.int32
    )
    running = jnp.cumsum(one_hot, axis=0)
    rank = jnp.sum((running - 1) * one_hot, axis=1)
    slot = flat_route * slot_cap + rank
    select = (slot[None, :] == jnp.arange(dest_count * slot_cap, dtype=jnp.int32)[:, None]).astype(
        jnp.bfloat16
    )
    pair_rows = jnp.repeat(ffn_in, top_count, axis=0)
    outgoing = (
        matmul(select, pair_rows).astype(jnp.bfloat16).reshape(dest_count, slot_cap, model_width)
    )
    arrived = lax.all_to_all(outgoing, "ep", split_axis=0, concat_axis=0, tiled=True)
    src_count, slot_items, width_in = arrived.shape
    flat_in = arrived.reshape(src_count * slot_items, width_in)
    expert_act = (silu_of(matmul(flat_in, expert_gate[0])) * matmul(flat_in, expert_up[0])).astype(
        jnp.bfloat16
    )
    result = matmul(expert_act, expert_down[0]).reshape(src_count, slot_items, width_in)
    returned = lax.all_to_all(
        result.astype(jnp.bfloat16), "ep", split_axis=0, concat_axis=0, tiled=True
    ).astype(result.dtype)
    per_pair = jnp.take(returned.reshape(dest_count * slot_cap, model_width), slot, axis=0)
    expert_sum = jnp.sum(
        per_pair.reshape(seq_count, top_count, model_width) * route_scale[:, :, None], axis=1
    )
    mixed = of_everyone(
        (expert_sum + blend[:, None] * dense_out).astype(jnp.bfloat16), "tp"
    ).astype(jnp.float32)
    layer_out = (first_res.astype(jnp.float32) + mixed).astype(jnp.bfloat16)
    return (layer_out, new_state)


def solution(mesh):
    in_specs = (
        P("ep", None),
        P(),
        P(None, "tp"),
        P(None, "tp"),
        P(None, "tp"),
        P(),
        P(),
        P(),
        P(),
        P(),
        P(),
        P(),
        P("tp", None),
        P("ep", "tp", None, None),
        P(),
        P(),
        P(None, ("ep", "tp")),
        P(None, ("ep", "tp")),
        P(("ep", "tp"), None),
        P("ep", None, "tp"),
        P("ep", None, "tp"),
        P("ep", "tp", None),
        P("ep", None),
        P("ep", None),
    )
    out_specs = (P("ep", None), P("ep", "tp", None, None))
    return jax.shard_map(shards, mesh=mesh, in_specs=in_specs, out_specs=out_specs, check_vma=False)
```

profile of v0, /device:TPU:1, one launch (start us, length us, event | category | flops | bytes accessed | tf_op | source)
XLA Modules:
  0.0 323.2 jit_solution(13139038705926091607)
XLA Ops:
  7.3 1.3 fusion.28
  9.3 1.5 fusion.21
  11.6 2.2 convolution_convert_fusion.4
  17.1 1.5 fusion.41
  19.4 2.1 convolution_convert_fusion.3
  22.3 2.1 convolution_convert_fusion.2
  26.5 10.2 %fusion.58 = f32[64,8,1,64]{3,2,1,0:T(1,128)S(1)} fusion(f32[64,8,64,1]{2,3,1,0:T(1,128)S(1)} %bitcast.78, f32[64,8,64,64]{3,2,1,0:T(8,128)} %param.37), kind=kOutput, calls=%fused_computation.89 | convolution fusion | flops 4194304 | bytes 8650752 | tf_op jit(solution)/shard_map/shij,shj->shi/dot_general | solution.py:81
  36.7 13.7 %multiply_add_fusion = f32[64,8,64,64]{3,2,1,0:T(8,128)} fusion(f32[64,8,64,64]{3,2,1,0:T(8,128)} %param.37, f32[64,8,64]{2,1,0:T(8,128)S(1)} %get-tuple-element.6, f32[64,8,64]{2,1,0:T(8,128)S(1)} %copy-done.7, f32[64,8,64]{2,1,0:T(8,128)S(1)} %get-tuple-element.4, f32[64,8,64]{2,1,0:T(8,128)S(1)} %bitcast.77, f32[64,8,64]{2,1,0:T(8,128)S(1)} %copy-done.8), kind=kLoop, calls=%fused_computation.1 | loop fusion | flops 10485760 | bytes 17432576 | tf_op jit(solution)/shard_map/add | solution.py:83
  50.4 10.9 %fusion.59 = f32[64,8,1,64]{3,2,1,0:T(1,128)} fusion(f32[64,8,64,64]{3,2,1,0:T(8,128)} %multiply_add_fusion, bf16[64,8,64,1]{2,3,1,0:T(2,128)(2,1)} %reshape.192), kind=kOutput, calls=%fused_computation.90 | convolution fusion | flops 4194304 | bytes 8585216 | tf_op jit(solution)/shard_map/shij,shj->shi/dot_general | solution.py:87
  66.9 2.1 convolution_convert_fusion.1
  69.1 5.2 %all_to_all.39 = bf16[2,64,2048]{2,1,0:T(8,128)(2,1)S(1)} all-to-all(bf16[2,64,2048]{2,1,0:T(8,128)(2,1)S(1)} %broadcast_in_dim.13), channel_id=1, replica_groups=mesh['ep'=64,'tp'=2] {'tp'}, dimensions={0} | all-to-all | bytes 1048576 | tf_op jit(solution)/shard_map/all_to_all | solution.py:9
  76.9 2.1 broadcast_in_dim.15
  79.0 2.0 reshape.164
  81.7 2.5 convolution_convert_fusion
  84.2 2.2 reshape.165
  86.5 11.7 %all-to-all-start.1 = ((bf16[64,4,2048]{2,1,0:T(4,128)(2,1)}), bf16[64,4,2048]{2,1,0:T(4,128)(2,1)}, u32[]{:S(2)}, u32[]{:S(2)}) async-start(bf16[64,4,2048]{2,1,0:T(4,128)(2,1)} %reshape.165), calls=%async_computation.1 | async-start | bytes 2097152 | tf_op jit(solution)/shard_map/all_to_all | solution.py:126
  100.2 16.2 %all-to-all-done.1 = bf16[64,4,2048]{2,1,0:T(4,128)(2,1)} async-done(((bf16[64,4,2048]{2,1,0:T(4,128)(2,1)}), bf16[64,4,2048]{2,1,0:T(4,128)(2,1)}, u32[]{:S(2)}, u32[]{:S(2)}) %all-to-all-start.1) | async-done | bytes 1048608 | tf_op jit(solution)/shard_map/all_to_all | solution.py:126
  116.4 2.2 reshape.166
  118.6 3.3 %fusion.5 = f32[256,768]{1,0:T(8,128)S(1)} fusion(bf16[256,2048]{1,0:T(8,128)(2,1)} %reshape.166, bf16[1,2048,768]{2,1,0:T(8,128)(2,1)} %param.43), kind=kOutput, calls=%fused_computation.8 | convolution fusion | flops 805306368 | bytes 4980736 | tf_op jit(solution)/shard_map/dot_general | solution.py:31
  123.9 2.0 fusion.7
  125.9 1.8 copy.54
  127.8 4.8 %all-to-all-start.2 = ((bf16[64,4,2048]{2,1,0:T(4,128)(2,1)}), bf16[64,4,2048]{2,1,0:T(4,128)(2,1)S(1)}, u32[]{:S(2)}, u32[]{:S(2)}) async-start(bf16[64,4,2048]{2,1,0:T(4,128)(2,1)} %copy.54), calls=%async_computation.2 | async-start | bytes 2097152 | tf_op jit(solution)/shard_map/all_to_all | solution.py:133
  132.6 63.2 %all-gather.4.cloned.1.call-done = bf16[4096,2048]{1,0:T(8,128)(2,1)} async-done(((bf16[64,2048]{1,0:T(8,128)(2,1)}), bf16[4096,2048]{1,0:T(8,128)(2,1)}) %all-gather.4.cloned.1.call-update) | async-done | bytes 16777232 | tf_op jit(solution)/shard_map/all_gather | solution.py:105
  195.8 11.1 %fusion.60 = f32[4096,44]{0,1:T(8,128)S(1)} fusion(bf16[4096,2048]{1,0:T(8,128)(2,1)} %all-gather.4.cloned.1.call-done, bf16[2048,44]{0,1:T(8,128)(2,1)S(1)} %copy-done.11), kind=kOutput, calls=%fused_computation.91 | convolution fusion | flops 738197504 | bytes 17678336 | tf_op jit(solution)/shard_map/dot_general | solution.py:31
  206.9 5.2 %fusion = bf16[4096,44]{0,1:T(8,128)(2,1)S(1)} fusion(bf16[4096,2048]{1,0:T(8,128)(2,1)S(1)} %copy-done.2, bf16[2048,44]{0,1:T(8,128)(2,1)S(1)} %copy-done.22, f32[4096,44]{0,1:T(8,128)S(1)} %fusion.60), kind=kOutput, calls=%fused_computation.3 | convolution fusion | flops 739098624 | bytes 18038784 | tf_op jit(solution)/shard_map/dot_general | solution.py:31
  213.4 1.2 reshape.194
  214.6 6.5 %all-to-all-start.3 = ((bf16[64,2,1408]{2,1,0:T(2,128)(2,1)}), bf16[64,2,1408]{2,1,0:T(2,128)(2,1)S(1)}, u32[]{:S(2)}, u32[]{:S(2)}) async-start(bf16[64,2,1408]{2,1,0:T(2,128)(2,1)} %reshape.194), calls=%async_computation.3 | async-start | bytes 720896 | tf_op jit(solution)/shard_map/all_to_all | solution.py:107
  222.9 3.1 multiply_reduce_fusion
  226.0 60.7 %all-gather.6.cloned.1.call-done = bf16[64,44,2048]{2,1,0:T(8,128)(2,1)} async-done(((bf16[1,44,2048]{2,1,0:T(8,128)(2,1)}), bf16[64,44,2048]{2,1,0:T(8,128)(2,1)}) %all-gather.6.cloned.1.call-update) | async-done | bytes 11534352 | tf_op jit(solution)/shard_map/all_gather | solution.py:108
  286.7 15.5 %reshape.183 = bf16[2816,2048]{1,0:T(8,128)(2,1)} reshape(bf16[64,44,2048]{2,1,0:T(8,128)(2,1)} %all-gather.6.cloned.1.call-done) | data formatting | bytes 23068672
  304.0 6.8 %fusion.11 = bf16[64,2048]{1,0:T(8,128)(2,1)S(1)} fusion(f32[64,2048]{1,0:T(8,128)} %multiply_reduce_fusion, bf16[64,2816]{0,1:T(8,128)(2,1)} %reshape.193, bf16[2816,2048]{1,0:T(8,128)(2,1)} %reshape.183, f32[64]{0:T(128)S(1)} %fusion.27), kind=kOutput, calls=%fused_computation.15 | convolution fusion | flops 738590720 | bytes 12681472 | tf_op jit(solution)/shard_map/dot_general | solution.py:31
  310.9 4.6 %all_to_all.40 = bf16[2,64,2048]{2,1,0:T(8,128)(2,1)S(1)} all-to-all(bf16[2,64,2048]{2,1,0:T(8,128)(2,1)S(1)} %broadcast_in_dim.17), channel_id=1, replica_groups=mesh['ep'=64,'tp'=2] {'tp'}, dimensions={0} | all-to-all | bytes 1048576 | tf_op jit(solution)/shard_map/all_to_all | solution.py:9
  (107 shorter events, 27.1 us)
Async XLA Ops:
  7.2 116.8 %copy-start = (bf16[1,768,2048]{2,1,0:T(8,128)(2,1)S(1)}, bf16[1,768,2048]{2,1,0:T(8,128)(2,1)}, u32[]{:S(2)}) copy-start(bf16[1,768,2048]{2,1,0:T(8,128)(2,1)} %param.45) | copy-start | bytes 9437188
  7.2 9.9 %copy-start.3 = (bf16[64,2048]{1,0:T(8,128)(2,1)S(1)}, bf16[64,2048]{1,0:T(8,128)(2,1)}, u32[]{:S(2)}) copy-start(bf16[64,2048]{1,0:T(8,128)(2,1)} %param.24) | copy-start | bytes 786436
  7.2 9.9 %copy-start.14 = (f32[2048]{0:T(1024)S(1)}, f32[2048]{0:T(1024)}, u32[]{:S(2)}) copy-start(f32[2048]{0:T(1024)} %param.25) | copy-start | bytes 24580
  7.2 188.6 %all-gather.4.cloned.1.call-start = ((), (), s32[]{:S(2)}) async-start(), calls=%async_computation.5 | async-start | bytes 17039360 | tf_op jit(solution)/shard_map/all_gather | solution.py:105
  19.4 5.9 %copy-start.13 = (f32[64,8]{1,0:T(8,128)S(1)}, f32[64,8]{1,0:T(8,128)}, u32[]{:S(2)}) copy-start(f32[64,8]{1,0:T(8,128)} %add_rsqrt_fusion.1) | copy-start | bytes 6148
  26.5 10.3 %copy-start.7 = (f32[64,8,64]{2,1,0:T(8,128)S(1)}, f32[64,8,64]{2,1,0:T(8,128)}, u32[]{:S(2)}) copy-start(f32[64,8,64]{2,1,0:T(8,128)} %reshape.171) | copy-start | bytes 393220
  26.5 10.2 %copy-start.8 = (f32[64,8,64]{2,1,0:T(8,128)S(1)}, f32[64,8,64]{2,1,0:T(8,128)}, u32[]{:S(2)}) copy-start(f32[64,8,64]{2,1,0:T(8,128)} %mul.187) | copy-start | bytes 393220
  50.4 14.4 %copy-start.19 = (f32[1024]{0:T(1024)S(1)}, f32[1024]{0:T(1024)}, u32[]{:S(2)}) copy-start(f32[1024]{0:T(1024)} %param.35) | copy-start | bytes 12292
  62.4 0.6 copy-start.10
  66.9 8.4 %copy-start.16 = (f32[2048]{0:T(1024)S(1)}, f32[2048]{0:T(1024)}, u32[]{:S(2)}) copy-start(f32[2048]{0:T(1024)} %param.38) | copy-start | bytes 24580
  69.1 11.9 %copy-start.15 = (s32[64,2]{0,1:T(2,128)S(1)}, s32[64,2]{0,1:T(2,128)}, u32[]{:S(2)}) copy-start(s32[64,2]{0,1:T(2,128)} %param.46) | copy-start | bytes 1540
  74.6 0.7 copy-start.5
  76.1 210.6 %all-gather.6.cloned.1.call-start = ((), (), s32[]{:S(2)}) async-start(), calls=%async_computation.6 | async-start | bytes 12779520 | tf_op jit(solution)/shard_map/all_gather | solution.py:108
  81.0 17.7 %copy-start.18 = (f32[64,2]{0,1:T(2,128)S(1)}, f32[64,2]{0,1:T(2,128)}, u32[]{:S(2)}) copy-start(f32[64,2]{0,1:T(2,128)} %param.47) | copy-start | bytes 1540
  81.0 18.4 %copy-start.17 = (bf16[2048]{0:T(1024)(128)(2,1)S(1)}, bf16[2048]{0:T(1024)(128)(2,1)}, u32[]{:S(2)}) copy-start(bf16[2048]{0:T(1024)(128)(2,1)} %param.39) | copy-start | bytes 12292
  81.0 19.0 %copy-start.4 = (bf16[64,2048]{1,0:T(8,128)(2,1)S(1)}, bf16[64,2048]{1,0:T(8,128)(2,1)}, u32[]{:S(2)}) copy-start(bf16[64,2048]{1,0:T(8,128)(2,1)} %fusion.34) | copy-start | bytes 786436
  86.5 30.0 %all-to-all-start.1 = ((bf16[64,4,2048]{2,1,0:T(4,128)(2,1)}), bf16[64,4,2048]{2,1,0:T(4,128)(2,1)}, u32[]{:S(2)}, u32[]{:S(2)}) async-start(bf16[64,4,2048]{2,1,0:T(4,128)(2,1)} %reshape.165), calls=%async_computation.1 | async-start | bytes 2097152 | tf_op jit(solution)/shard_map/all_to_all | solution.py:126
  118.6 3.3 %copy-start.9 = (bf16[256,2048]{1,0:T(8,128)(2,1)S(1)}, bf16[256,2048]{1,0:T(8,128)(2,1)}, u32[]{:S(2)}) copy-start(bf16[256,2048]{1,0:T(8,128)(2,1)} %reshape.166) | copy-start | bytes 3145732
  118.6 3.5 %copy-start.21 = (bf16[1,2048,768]{2,1,0:T(8,128)(2,1)S(1)}, bf16[1,2048,768]{2,1,0:T(8,128)(2,1)}, u32[]{:S(2)}) copy-start(bf16[1,2048,768]{2,1,0:T(8,128)(2,1)} %param.44) | copy-start | bytes 9437188
  125.9 69.9 %copy-start.11 = (bf16[2048,44]{0,1:T(8,128)(2,1)S(1)}, bf16[2048,44]{0,1:T(8,128)(2,1)}, u32[]{:S(2)}) copy-start(bf16[2048,44]{0,1:T(8,128)(2,1)} %param.40) | copy-start | bytes 540676
  127.8 86.8 %all-to-all-start.2 = ((bf16[64,4,2048]{2,1,0:T(4,128)(2,1)}), bf16[64,4,2048]{2,1,0:T(4,128)(2,1)S(1)}, u32[]{:S(2)}, u32[]{:S(2)}) async-start(bf16[64,4,2048]{2,1,0:T(4,128)(2,1)} %copy.54), calls=%async_computation.2 | async-start | bytes 2097152 | tf_op jit(solution)/shard_map/all_to_all | solution.py:133
  132.6 74.3 %copy-start.22 = (bf16[2048,44]{0,1:T(8,128)(2,1)S(1)}, bf16[2048,44]{0,1:T(8,128)(2,1)}, u32[]{:S(2)}) copy-start(bf16[2048,44]{0,1:T(8,128)(2,1)} %param.41) | copy-start | bytes 540676
  195.8 11.1 %copy-start.2 = (bf16[4096,2048]{1,0:T(8,128)(2,1)S(1)}, bf16[4096,2048]{1,0:T(8,128)(2,1)}, u32[]{:S(2)}) copy-start(bf16[4096,2048]{1,0:T(8,128)(2,1)} %all-gather.4.cloned.1.call-done) | copy-start | bytes 50331652
  212.1 9.0 %copy-start.20 = (s32[128]{0:T(128)S(1)}, s32[128]{0:T(128)}, u32[]{:S(2)}) copy-start(s32[128]{0:T(128)} %fusion.46) | copy-start | bytes 1540
  214.6 87.6 %all-to-all-start.3 = ((bf16[64,2,1408]{2,1,0:T(2,128)(2,1)}), bf16[64,2,1408]{2,1,0:T(2,128)(2,1)S(1)}, u32[]{:S(2)}, u32[]{:S(2)}) async-start(bf16[64,2,1408]{2,1,0:T(2,128)(2,1)} %reshape.194), calls=%async_computation.3 | async-start | bytes 720896 | tf_op jit(solution)/shard_map/all_to_all | solution.py:107
  221.3 1.6 copy-start.12
  304.0 11.6 %copy-start.6 = (bf16[64,2048]{1,0:T(8,128)(2,1)S(1)}, bf16[64,2048]{1,0:T(8,128)(2,1)}, u32[]{:S(2)}) copy-start(bf16[64,2048]{1,0:T(8,128)(2,1)} %copy-done.5) | copy-start | bytes 786436
  304.0 12.4 %copy-start.1 = (bf16[1,768,2048]{2,1,0:T(8,128)(2,1)S(1)}, bf16[1,768,2048]{2,1,0:T(8,128)(2,1)}, u32[]{:S(2)}) copy-start(bf16[1,768,2048]{2,1,0:T(8,128)(2,1)} %param.45) | copy-start | bytes 9437188
Sparse Core Ops, SparseCore 0:
  76.3 119.5 all-gather.3
  198.6 88.0 all-gather.5
where the time goes:
time: 325 us; the launch traced here: 323 us
  waiting for transfers between devices  141 us (43%)
  matrix products  64.8 us (20%)
  local copies, waits for them, and re-layouts  42.3 us (13%)
  other arithmetic  27.9 us (9%)
  starting transfers between devices  23.1 us (7%)
  between operations  14.5 us (4%)
  blocking collectives  9.79 us (3%)
    all_gather x1, waiting for transfers between devices, shards(): piece = lax.all_gather(ffn_in, 'ep', axis=0, tiled=True)  63.2 us
    all_gather x1, waiting for transfers between devices, shards(): lax.all_gather(dense_down, 'ep', axis=0, tiled=True)  60.7 us
    dot_general x13, matrix products, matmul(): return jnp.dot(left, right, preferred_element_type=jnp.float32)  43.4 us
    unnamed x52, local copies, waits for them, and re-layouts  19.6 us
    all_to_all x1, waiting for transfers between devices, shards(): lax.all_to_all(outgoing, 'ep', split_axis=0, concat_axis=0, tiled=True)  16.2 us
    add x1, other arithmetic, shards(): memory_state * decay_rate[:, :, None, :]  13.7 us
    all_to_all x1, starting transfers between devices, shards(): lax.all_to_all(outgoing, 'ep', split_axis=0, concat_axis=0, tiled=True)  11.7 us
    dot_general x1, matrix products, shards(): readout = jnp.einsum('shij,shj->shi', new_state, recept_rows)  10.9 us
  transfers between devices with their start and end apart: 5, of which 3 were waited for; matrix products, arithmetic and copies ran while one was open for 19% of the time, Pallas kernels for 0%

commit v1 on v0

--- a/solution.py
+++ b/solution.py
@@ -1,7 +1,116 @@
 import jax
 import jax.numpy as jnp
 from jax import lax
+from jax.experimental import pallas as pl
+from jax.experimental.pallas import tpu as pltpu
 from jax.sharding import PartitionSpec as P
+
+SB = 8
+
+
+def att_kernel(
+    hid_ref, mixg_ref, wr_ref, wk_ref, wv_ref, dd_ref, du_ref, db_ref, rd_ref, ru_ref, rb_ref, hg_ref, ow_ref,
+    st_ref, ns_ref, gp_ref, k_s, d_s, l_s, q_s, v_s, b_s, yt_s,
+):
+    step = pl.program_id(0)
+    heads, size = 8, 64
+    width = heads * size
+
+    @pl.when(step == 0)
+    def _():
+        own = pl.ds(pl.multiple_of(lax.axis_index("tp") * width, width), width)
+        x = hid_ref[...].astype(jnp.float32)
+        scale = lax.rsqrt(jnp.mean(x * x, axis=-1, keepdims=True) + 1e-06)
+        nb = (x * scale * mixg_ref[...]).astype(jnp.bfloat16)
+        low = jnp.tanh(nt_dot(nb, dd_ref[...])).astype(jnp.bfloat16)
+        pre = dot(low, du_ref[:, own]) + db_ref[:, own]
+        dec = jnp.exp(-jnp.exp(-0.5) * (1.0 / (1.0 + jnp.exp(-pre))))
+        rlow = nt_dot(nb, rd_ref[...]).astype(jnp.bfloat16)
+        lr = 1.0 / (1.0 + jnp.exp(-(dot(rlow, ru_ref[:, own]) + rb_ref[:, own])))
+        key = dot(nb, wk_ref[...]).astype(jnp.bfloat16).astype(jnp.float32)
+        val = dot(nb, wv_ref[...]).astype(jnp.bfloat16).astype(jnp.float32)
+        rec = dot(nb, wr_ref[...]).astype(jnp.bfloat16).astype(jnp.float32)
+        for h in range(heads):
+            cut = slice(h * size, (h + 1) * size)
+            kh, dh, lh, rh = key[:, cut], dec[:, cut], lr[:, cut], rec[:, cut]
+            rn2 = 1.0 / (jnp.sum(kh * kh, axis=-1, keepdims=True) + 1e-06)
+            kl = kh * lh
+            k_s[h] = kh * rn2
+            d_s[h] = dh
+            l_s[h] = kl
+            q_s[h] = dh * rh
+            v_s[h] = val[:, cut]
+            b_s[h] = jnp.broadcast_to(jnp.sum(kl * rh, axis=-1, keepdims=True), (64, size))
+
+    eye = (
+        lax.broadcasted_iota(jnp.int32, (size, size), 0) == lax.broadcasted_iota(jnp.int32, (size, size), 1)
+    )
+    lane = lax.broadcasted_iota(jnp.int32, (size, 128), 1)
+
+    def one(j, _):
+        for u in range(2):
+            sl = j * 2 + u
+            s = step * SB + sl
+            row = pl.ds(s, 1)
+            for h in range(heads):
+                m = st_ref[sl, h]
+                t = jnp.where(eye, v_s[h, row, :], 0.0) - m * k_s[h, row, :]
+                w = jnp.sum(t, axis=-1, keepdims=True)
+                y0 = jnp.sum(m * q_s[h, row, :], axis=-1, keepdims=True)
+                ns_ref[sl, h] = m * d_s[h, row, :] + w * l_s[h, row, :]
+                y = y0 + w * b_s[h, row, 0:1]
+                yt_s[h] = jnp.where(lane == s, y, yt_s[h])
+        return 0
+
+    lax.fori_loop(0, SB // 2, one, 0)
+
+    @pl.when(step == pl.num_programs(0) - 1)
+    def _():
+        parts = []
+        for h in range(heads):
+            y = yt_s[h]
+            c = y - jnp.mean(y, axis=0, keepdims=True)
+            var = jnp.mean(c * c, axis=0, keepdims=True)
+            parts.append(c * lax.rsqrt(var + 0.00064))
+        full = jnp.concatenate(parts, axis=0).T[:64]
+        hn = (full * hg_ref[:, pl.ds(pl.multiple_of(lax.axis_index("tp") * width, width), width)]).astype(jnp.bfloat16)
+        gp_ref[...] = dot(hn, ow_ref[...]).astype(jnp.bfloat16)
+
+
+def dot(a, b):
+    return jnp.dot(a, b, preferred_element_type=jnp.float32)
+
+
+def nt_dot(a, b):
+    return lax.dot_general(a, b, (((1,), (1,)), ((), ())), preferred_element_type=jnp.float32)
+
+
+def attention(hidden, mix_gain, wr, wk, wv, dd, du, db, rd, ru, rb, hg, ow, state):
+    seqs = hidden.shape[0]
+    whole = lambda shape: pl.BlockSpec(shape, lambda g: tuple(0 for _ in shape))
+    ops = [
+        hidden, mix_gain.reshape(1, -1), wr, wk, wv, dd.T, du, db.reshape(1, -1), rd.T, ru, rb.reshape(1, -1),
+        hg.reshape(1, -1), ow,
+    ]
+    blk = pl.BlockSpec((SB, 8, 64, 64), lambda g: (g, 0, 0, 0))
+    small = pltpu.VMEM((8, seqs, 64), jnp.float32)
+    new_state, part = pl.pallas_call(
+        att_kernel,
+        grid=(seqs // SB,),
+        in_specs=[whole(o.shape) for o in ops] + [blk],
+        out_specs=[blk, whole((seqs, 2048))],
+        out_shape=[
+            jax.ShapeDtypeStruct(state.shape, jnp.float32),
+            jax.ShapeDtypeStruct((seqs, 2048), jnp.bfloat16),
+        ],
+        scratch_shapes=[small] * 6 + [pltpu.VMEM((8, 64, 128), jnp.float32)],
+        compiler_params=pltpu.CompilerParams(
+            dimension_semantics=("arbitrary",), vmem_limit_bytes=60 * 1024 * 1024
+        ),
+        cost_estimate=pl.CostEstimate(flops=40_000_000_000, bytes_accessed=44_000_000, transcendentals=0),
+        name="attention",
+    )(*ops, state)
+    return new_state, part
 
 
 def copy_for_each(x, axis):
@@ -58,45 +167,11 @@
     route_scale,
 ):
     seq_count, model_width = hidden.shape
-    own_width = recept_weight.shape[1]
-    head_count = memory_state.shape[1]
-    head_size = memory_state.shape[2]
-    offset = lax.axis_index("tp") * own_width
-    decay_up_own = lax.dynamic_slice_in_dim(decay_up, offset, own_width, 1)
-    rate_up_own = lax.dynamic_slice_in_dim(rate_up, offset, own_width, 1)
-    decay_bias_own = lax.dynamic_slice_in_dim(decay_bias, offset, own_width, 0)
-    rate_bias_own = lax.dynamic_slice_in_dim(rate_bias, offset, own_width, 0)
-    gain_own = lax.dynamic_slice_in_dim(head_gain, offset, own_width, 0)
-    normed_in = rms_scaled(hidden, mix_gain).astype(jnp.bfloat16)
-    split_shape = (seq_count, head_count, head_size)
-    recept_rows = stored(matmul(normed_in, recept_weight)).reshape(split_shape)
-    key_rows = stored(matmul(normed_in, key_weight)).reshape(split_shape)
-    value_rows = stored(matmul(normed_in, value_weight)).reshape(split_shape)
-    decay_low = jnp.tanh(matmul(normed_in, decay_down)).astype(jnp.bfloat16)
-    decay_pre = matmul(decay_low, decay_up_own) + decay_bias_own
-    decay_rate = jnp.exp(-jnp.exp(-jax.nn.softplus(-decay_pre) - 0.5)).reshape(split_shape)
-    rate_low = matmul(normed_in, rate_down).astype(jnp.bfloat16)
-    learn_rate = jax.nn.sigmoid(matmul(rate_low, rate_up_own) + rate_bias_own).reshape(split_shape)
-    unit_key = key_rows * lax.rsqrt(jnp.sum(key_rows * key_rows, axis=-1, keepdims=True) + 1e-06)
-    removed = jnp.einsum("shij,shj->shi", memory_state, unit_key)
-    new_state = (
-        memory_state * decay_rate[:, :, None, :]
-        - removed[..., None] * (unit_key * learn_rate)[:, :, None, :]
-        + value_rows[..., None] * (key_rows * learn_rate)[:, :, None, :]
-    )
-    readout = jnp.einsum("shij,shj->shi", new_state, recept_rows)
-    centre = jnp.mean(readout, axis=-1, keepdims=True)
-    variance = jnp.mean(jnp.square(readout - centre), axis=-1, keepdims=True)
-    head_normed = (
-        (
-            (readout - centre)
-            * lax.rsqrt(variance + 0.00064)
-            * gain_own.reshape(head_count, head_size)
-        )
-        .astype(jnp.bfloat16)
-        .reshape(seq_count, own_width)
-    )
-    attn_sum = of_everyone(matmul(head_normed, out_weight).astype(jnp.bfloat16), "tp").astype(
+    new_state, part = attention(
+        hidden, mix_gain, recept_weight, key_weight, value_weight, decay_down, decay_up, decay_bias,
+        rate_down, rate_up, rate_bias, head_gain, out_weight, memory_state,
+    )
+    attn_sum = of_everyone(part, "tp").astype(
         jnp.float32
     )
     first_res = (hidden.astype(jnp.float32) + attn_sum).astype(jnp.bfloat16)

time: 325 us -> 297 us (0.914)
  matrix products: 64.8 us -> 32 us
  Pallas kernels: 0 us -> 27 us
  other arithmetic: 27.9 us -> 7.19 us
  waiting for transfers between devices: 141 us -> 129 us
  local copies, waits for them, and re-layouts: 42.3 us -> 51.8 us
    pallas_call x0 -> x1, Pallas kernels: none -> 27 us  [attention(): pl.pallas_call(att_kernel, grid=(seqs // SB,), in_specs=[whole(o.shape) f...]
    dot_general x2 -> x0, matrix products: 21.1 us -> none  [the longest x1 10.9 us: shards(): readout = jnp.einsum('shij,shj->shi', new_state, recept_rows)]
    add x1 -> x0, other arithmetic: 13.7 us -> none  [shards(): memory_state * decay_rate[:, :, None, :]]
    dot_general x13 -> x7, matrix products: 43.4 us -> 31.8 us  [matmul(): return jnp.dot(left, right, preferred_element_type=jnp.float32)]
    all_gather x1, waiting for transfers between devices: 60.7 us -> 49.8 us  [shards(): lax.all_gather(dense_down, 'ep', axis=0, tiled=True)]
    all_to_all x4, local copies, waits for them, and re-layouts: 2.42 us -> 8.35 us  [shards(): lax.all_to_all(dense_act, 'ep', split_axis=0, concat_axis=1, tiled=True)]
    gather x2, local copies, waits for them, and re-layouts: 1.6 us -> 6.85 us  [shards(): jnp.take(returned.reshape(dest_count * slot_cap, model_width), slot, axis=0)]
    reduce_sum x3 -> x0, other arithmetic: 3.35 us -> none  [the longest x1 1.17 us: shards(): variance = jnp.mean(jnp.square(readout - centre), axis=-1, keepdims=True)]
  transfers between devices with their start and end apart: 5 -> 5, of which waited for: 3 -> 3; matrix products, arithmetic and copies ran while one was open for 19% -> 25% of each run, Pallas kernels for 0% -> 0%
where the time goes in v1:
time: 297 us; the launch traced here: 296 us
  waiting for transfers between devices  129 us (43%)
  local copies, waits for them, and re-layouts  51.8 us (17%)
  matrix products  32 us (11%)
  Pallas kernels  27 us (9%)
  starting transfers between devices  24 us (8%)
  between operations  14.3 us (5%)
  blocking collectives  9.78 us (3%)
  other arithmetic  7.19 us (2%)
    all_gather x1, waiting for transfers between devices, shards(): piece = lax.all_gather(ffn_in, 'ep', axis=0, tiled=True)  62.6 us
    all_gather x1, waiting for transfers between devices, shards(): lax.all_gather(dense_down, 'ep', axis=0, tiled=True)  49.8 us
    dot_general x7, matrix products, matmul(): return jnp.dot(left, right, preferred_element_type=jnp.float32)  31.8 us
    pallas_call x1, Pallas kernels, attention(): pl.pallas_call(att_kernel, grid=(seqs // SB,), in_specs=[whole(o.shape) f...  27 us
    unnamed x38, local copies, waits for them, and re-layouts  21.3 us
    all_to_all x1, waiting for transfers between devices, shards(): lax.all_to_all(outgoing, 'ep', split_axis=0, concat_axis=0, tiled=True)  16.2 us
    all_to_all x1, starting transfers between devices, shards(): lax.all_to_all(outgoing, 'ep', split_axis=0, concat_axis=0, tiled=True)  11.5 us
    all_to_all x2, blocking collectives, copy_for_each(): lax.all_to_all(jnp.broadcast_to(x[None], (length, *x.shape)), axis, 0, 0,...  9.78 us
  transfers between devices with their start and end apart: 5, of which 3 were waited for; matrix products, arithmetic and copies ran while one was open for 25% of the time, Pallas kernels for 0%

profile of v1, /device:TPU:1, one launch (start us, length us, event | category | flops | bytes accessed | tf_op | source)
XLA Modules:
  0.0 295.5 jit_solution(13286376599324104440)
XLA Ops:
  7.2 27.0 %attention.1 = (f32[64,8,64,64]{3,2,1,0:T(8,128)}, bf16[64,2048]{1,0:T(8,128)(2,1)}) custom-call(bf16[64,2048]{1,0:T(8,128)(2,1)} %hid_ref.1, f32[1,2048]{1,0:T(1,128)} %bitcast.65, bf16[2048,512]{1,0:T(8,128)(2,1)} %wr_ref.1, bf16[2048,512]{1,0:T(8,128)(2,1)} %wk_ref.1, bf16[2048,512]{1,0:T(8,128)(2,1)} %wv_ref.1, bf16[64,2048]{1,0:T(8,128)(2,1)} %bitcast.63, ...), custom_call_target="tpu_custom_call" | custom-call | flops 40000000000 | bytes 44000000 | tf_op jit(solution)/shard_map/attention/pallas_call | solution.py:97
  35.3 5.2 %all_to_all.39 = bf16[2,64,2048]{2,1,0:T(8,128)(2,1)S(1)} all-to-all(bf16[2,64,2048]{2,1,0:T(8,128)(2,1)S(1)} %broadcast_in_dim.16), channel_id=1, replica_groups=mesh['ep'=64,'tp'=2] {'tp'}, dimensions={0} | all-to-all | bytes 1048576 | tf_op jit(solution)/shard_map/all_to_all | solution.py:118
  43.3 2.1 broadcast_in_dim.18
  45.4 2.0 reshape.108
  47.9 2.5 convolution_convert_fusion
  50.4 2.2 reshape.109
  52.6 11.5 %all-to-all-start.1 = ((bf16[64,4,2048]{2,1,0:T(4,128)(2,1)}), bf16[64,4,2048]{2,1,0:T(4,128)(2,1)}, u32[]{:S(2)}, u32[]{:S(2)}) async-start(bf16[64,4,2048]{2,1,0:T(4,128)(2,1)} %reshape.109), calls=%async_computation.1 | async-start | bytes 2097152 | tf_op jit(solution)/shard_map/all_to_all | solution.py:201
  66.3 16.2 %all-to-all-done.1 = bf16[64,4,2048]{2,1,0:T(4,128)(2,1)} async-done(((bf16[64,4,2048]{2,1,0:T(4,128)(2,1)}), bf16[64,4,2048]{2,1,0:T(4,128)(2,1)}, u32[]{:S(2)}, u32[]{:S(2)}) %all-to-all-start.1) | async-done | bytes 1048608 | tf_op jit(solution)/shard_map/all_to_all | solution.py:201
  82.5 2.1 reshape.110
  84.6 3.3 %fusion.5 = f32[256,768]{1,0:T(8,128)S(1)} fusion(bf16[256,2048]{1,0:T(8,128)(2,1)} %reshape.110, bf16[1,2048,768]{2,1,0:T(8,128)(2,1)} %param.43), kind=kOutput, calls=%fused_computation.7 | convolution fusion | flops 805306368 | bytes 4980736 | tf_op jit(solution)/shard_map/dot_general | solution.py:140
  88.1 1.0 fusion.15
  90.0 2.0 fusion.7
  92.0 1.8 copy.54
  93.8 5.7 %all-to-all-start.2 = ((bf16[64,4,2048]{2,1,0:T(4,128)(2,1)}), bf16[64,4,2048]{2,1,0:T(4,128)(2,1)}, u32[]{:S(2)}, u32[]{:S(2)}) async-start(bf16[64,4,2048]{2,1,0:T(4,128)(2,1)} %copy.54), calls=%async_computation.2 | async-start | bytes 2097152 | tf_op jit(solution)/shard_map/all_to_all | solution.py:208
  99.5 62.6 %all-gather.4.cloned.1.call-done = bf16[4096,2048]{1,0:T(8,128)(2,1)} async-done(((bf16[64,2048]{1,0:T(8,128)(2,1)}), bf16[4096,2048]{1,0:T(8,128)(2,1)}) %all-gather.4.cloned.1.call-update) | async-done | bytes 16777232 | tf_op jit(solution)/shard_map/all_gather | solution.py:180
  162.1 11.1 %fusion.30 = f32[4096,44]{0,1:T(8,128)S(1)} fusion(bf16[4096,2048]{1,0:T(8,128)(2,1)} %all-gather.4.cloned.1.call-done, bf16[2048,44]{0,1:T(8,128)(2,1)S(1)} %copy-done.7), kind=kOutput, calls=%fused_computation.49 | convolution fusion | flops 738197504 | bytes 17678336 | tf_op jit(solution)/shard_map/dot_general | solution.py:140
  173.2 5.2 %fusion = bf16[4096,44]{0,1:T(8,128)(2,1)S(1)} fusion(bf16[4096,2048]{1,0:T(8,128)(2,1)S(1)} %copy-done.1, bf16[2048,44]{0,1:T(8,128)(2,1)S(1)} %copy-done.15, f32[4096,44]{0,1:T(8,128)S(1)} %fusion.30), kind=kOutput, calls=%fused_computation.2 | convolution fusion | flops 739098624 | bytes 18038784 | tf_op jit(solution)/shard_map/dot_general | solution.py:140
  178.4 1.6 all_to_all.29
  180.0 2.5 copy.63
  182.5 2.7 reshape.129
  185.2 6.7 %all-to-all-start.3 = ((bf16[64,2,1408]{2,1,0:T(2,128)(2,1)}), bf16[64,2,1408]{2,1,0:T(2,128)(2,1)S(1)}, u32[]{:S(2)}, u32[]{:S(2)}) async-start(bf16[64,2,1408]{2,1,0:T(2,128)(2,1)} %reshape.129), calls=%async_computation.3 | async-start | bytes 720896 | tf_op jit(solution)/shard_map/all_to_all | solution.py:182
  192.0 2.5 reshape.114
  194.4 4.0 %gather_fusion = f32[128,2048]{1,0:T(8,128)} fusion(f32[256,2048]{1,0:T(8,128)} %reshape.114, s32[1024]{0:T(1024)S(1)} %pad_clamp_fusion), kind=kCustom, calls=%fused_computation | custom fusion | bytes 2097664 | tf_op jit(solution)/shard_map/jit(_take)/gather | solution.py:211
  198.4 2.9 gather.7
  201.3 4.2 %multiply_reduce_fusion = f32[64,2048]{1,0:T(8,128)} fusion(f32[64,2,2048]{2,1,0:T(2,128)} %gather.7, pred[64,2]{1,0:T(8,128)(4,1)S(1)} %copy.52, f32[64,2]{1,0:T(8,128)S(1)} %copy-done.8), kind=kLoop, calls=%fused_computation.22 | loop fusion | flops 655360 | bytes 1573504 | tf_op jit(solution)/shard_map/reduce_sum | solution.py:212
  205.5 49.8 %all-gather.6.cloned.1.call-done = bf16[64,44,2048]{2,1,0:T(8,128)(2,1)} async-done(((bf16[1,44,2048]{2,1,0:T(8,128)(2,1)}), bf16[64,44,2048]{2,1,0:T(8,128)(2,1)}) %all-gather.6.cloned.1.call-update) | async-done | bytes 11534352 | tf_op jit(solution)/shard_map/all_gather | solution.py:183
  255.2 15.5 %reshape.124 = bf16[2816,2048]{1,0:T(8,128)(2,1)} reshape(bf16[64,44,2048]{2,1,0:T(8,128)(2,1)} %all-gather.6.cloned.1.call-done) | data formatting | bytes 23068672
  270.7 1.4 reshape.130
  272.2 2.1 bitcast_bitcast_fusion
  274.2 2.2 reshape.128
  276.4 6.7 %fusion.11 = bf16[64,2048]{1,0:T(8,128)(2,1)S(1)} fusion(f32[64,2048]{1,0:T(8,128)} %multiply_reduce_fusion, bf16[64,2816]{0,1:T(8,128)(2,1)} %reshape.128, bf16[2816,2048]{1,0:T(8,128)(2,1)} %reshape.124, f32[64]{0:T(128)S(1)} %fusion.21), kind=kOutput, calls=%fused_computation.13 | convolution fusion | flops 738590720 | bytes 12681472 | tf_op jit(solution)/shard_map/dot_general | solution.py:140
  283.2 4.6 %all_to_all.40 = bf16[2,64,2048]{2,1,0:T(8,128)(2,1)S(1)} all-to-all(bf16[2,64,2048]{2,1,0:T(8,128)(2,1)S(1)} %broadcast_in_dim.20), channel_id=1, replica_groups=mesh['ep'=64,'tp'=2] {'tp'}, dimensions={0} | all-to-all | bytes 1048576 | tf_op jit(solution)/shard_map/all_to_all | solution.py:118
  (65 shorter events, 8.3 us)
Async XLA Ops:
  7.2 82.8 %copy-start = (bf16[1,768,2048]{2,1,0:T(8,128)(2,1)S(1)}, bf16[1,768,2048]{2,1,0:T(8,128)(2,1)}, u32[]{:S(2)}) copy-start(bf16[1,768,2048]{2,1,0:T(8,128)(2,1)} %param.45) | copy-start | bytes 9437188
  7.2 155.0 %all-gather.4.cloned.1.call-start = ((), (), s32[]{:S(2)}) async-start(), calls=%async_computation.5 | async-start | bytes 17039360 | tf_op jit(solution)/shard_map/all_gather | solution.py:180
  7.2 33.3 %copy-start.6 = (bf16[64,2048]{1,0:T(8,128)(2,1)S(1)}, bf16[64,2048]{1,0:T(8,128)(2,1)}, u32[]{:S(2)}) copy-start(bf16[64,2048]{1,0:T(8,128)(2,1)} %hid_ref.1) | copy-start | bytes 786436
  34.2 7.2 %copy-start.10 = (f32[2048]{0:T(1024)S(1)}, f32[2048]{0:T(1024)}, u32[]{:S(2)}) copy-start(f32[2048]{0:T(1024)} %param.38) | copy-start | bytes 24580
  34.2 8.8 %copy-start.9 = (s32[64,2]{0,1:T(2,128)S(1)}, s32[64,2]{0,1:T(2,128)}, u32[]{:S(2)}) copy-start(s32[64,2]{0,1:T(2,128)} %param.46) | copy-start | bytes 1540
  40.7 0.7 copy-start.3
  42.3 212.9 %all-gather.6.cloned.1.call-start = ((), (), s32[]{:S(2)}) async-start(), calls=%async_computation.6 | async-start | bytes 12779520 | tf_op jit(solution)/shard_map/all_gather | solution.py:183
  47.4 17.3 %copy-start.12 = (f32[64,2]{0,1:T(2,128)S(1)}, f32[64,2]{0,1:T(2,128)}, u32[]{:S(2)}) copy-start(f32[64,2]{0,1:T(2,128)} %param.47) | copy-start | bytes 1540
  47.4 18.1 %copy-start.11 = (bf16[2048]{0:T(1024)(128)(2,1)S(1)}, bf16[2048]{0:T(1024)(128)(2,1)}, u32[]{:S(2)}) copy-start(bf16[2048]{0:T(1024)(128)(2,1)} %param.39) | copy-start | bytes 12292
  47.4 18.7 %copy-start.2 = (bf16[64,2048]{1,0:T(8,128)(2,1)S(1)}, bf16[64,2048]{1,0:T(8,128)(2,1)}, u32[]{:S(2)}) copy-start(bf16[64,2048]{1,0:T(8,128)(2,1)} %fusion.24) | copy-start | bytes 786436
  52.6 29.9 %all-to-all-start.1 = ((bf16[64,4,2048]{2,1,0:T(4,128)(2,1)}), bf16[64,4,2048]{2,1,0:T(4,128)(2,1)}, u32[]{:S(2)}, u32[]{:S(2)}) async-start(bf16[64,4,2048]{2,1,0:T(4,128)(2,1)} %reshape.109), calls=%async_computation.1 | async-start | bytes 2097152 | tf_op jit(solution)/shard_map/all_to_all | solution.py:201
  84.6 3.3 %copy-start.5 = (bf16[256,2048]{1,0:T(8,128)(2,1)S(1)}, bf16[256,2048]{1,0:T(8,128)(2,1)}, u32[]{:S(2)}) copy-start(bf16[256,2048]{1,0:T(8,128)(2,1)} %reshape.110) | copy-start | bytes 3145732
  84.6 3.5 %copy-start.14 = (bf16[1,2048,768]{2,1,0:T(8,128)(2,1)S(1)}, bf16[1,2048,768]{2,1,0:T(8,128)(2,1)}, u32[]{:S(2)}) copy-start(bf16[1,2048,768]{2,1,0:T(8,128)(2,1)} %param.44) | copy-start | bytes 9437188
  92.0 70.1 %copy-start.7 = (bf16[2048,44]{0,1:T(8,128)(2,1)S(1)}, bf16[2048,44]{0,1:T(8,128)(2,1)}, u32[]{:S(2)}) copy-start(bf16[2048,44]{0,1:T(8,128)(2,1)} %param.40) | copy-start | bytes 540676
  93.8 91.4 %all-to-all-start.2 = ((bf16[64,4,2048]{2,1,0:T(4,128)(2,1)}), bf16[64,4,2048]{2,1,0:T(4,128)(2,1)}, u32[]{:S(2)}, u32[]{:S(2)}) async-start(bf16[64,4,2048]{2,1,0:T(4,128)(2,1)} %copy.54), calls=%async_computation.2 | async-start | bytes 2097152 | tf_op jit(solution)/shard_map/all_to_all | solution.py:208
  162.1 11.1 %copy-start.1 = (bf16[4096,2048]{1,0:T(8,128)(2,1)S(1)}, bf16[4096,2048]{1,0:T(8,128)(2,1)}, u32[]{:S(2)}) copy-start(bf16[4096,2048]{1,0:T(8,128)(2,1)} %all-gather.4.cloned.1.call-done) | copy-start | bytes 50331652
  162.1 11.1 %copy-start.15 = (bf16[2048,44]{0,1:T(8,128)(2,1)S(1)}, bf16[2048,44]{0,1:T(8,128)(2,1)}, u32[]{:S(2)}) copy-start(bf16[2048,44]{0,1:T(8,128)(2,1)} %param.41) | copy-start | bytes 540676
  180.0 11.9 %copy-start.13 = (s32[128]{0:T(128)S(1)}, s32[128]{0:T(128)}, u32[]{:S(2)}) copy-start(s32[128]{0:T(128)} %fusion.29) | copy-start | bytes 1540
  185.2 85.5 %all-to-all-start.3 = ((bf16[64,2,1408]{2,1,0:T(2,128)(2,1)}), bf16[64,2,1408]{2,1,0:T(2,128)(2,1)S(1)}, u32[]{:S(2)}, u32[]{:S(2)}) async-start(bf16[64,2,1408]{2,1,0:T(2,128)(2,1)} %reshape.129), calls=%async_computation.3 | async-start | bytes 720896 | tf_op jit(solution)/shard_map/all_to_all | solution.py:182
  194.4 6.9 %copy-start.8 = (f32[64,2]{1,0:T(8,128)S(1)}, f32[64,2]{1,0:T(8,128)}, u32[]{:S(2)}) copy-start(f32[64,2]{1,0:T(8,128)} %copy.56) | copy-start | bytes 1540
  276.4 11.5 %copy-start.4 = (bf16[64,2048]{1,0:T(8,128)(2,1)S(1)}, bf16[64,2048]{1,0:T(8,128)(2,1)}, u32[]{:S(2)}) copy-start(bf16[64,2048]{1,0:T(8,128)(2,1)} %copy-done.3) | copy-start | bytes 786436
Sparse Core Ops, SparseCore 0:
  42.4 119.6 all-gather.3
  164.9 90.2 all-gather.5

commit v2 on v1

--- a/solution.py
+++ b/solution.py
@@ -5,6 +5,7 @@
 from jax.experimental.pallas import tpu as pltpu
 from jax.sharding import PartitionSpec as P
 
+MESH = pl.DeviceIdType.MESH
 SB = 8
 
 
@@ -113,109 +114,253 @@
     return new_state, part
 
 
-def copy_for_each(x, axis):
-    length = lax.axis_size(axis)
-    return lax.all_to_all(jnp.broadcast_to(x[None], (length, *x.shape)), axis, 0, 0, tiled=True)
-
-
-def of_everyone(x, axis):
-    everything = copy_for_each(x, axis)
-    return jnp.sum(everything.astype(jnp.float32), axis=0)
-
-
-def stored(tensor):
-    return lax.optimization_barrier(tensor.astype(jnp.bfloat16)).astype(jnp.float32)
-
-
-def rms_scaled(tensor, gain_vec):
-    values = tensor.astype(jnp.float32)
-    return values * lax.rsqrt(jnp.mean(values * values, axis=-1, keepdims=True) + 1e-06) * gain_vec
-
-
-def silu_of(tensor):
-    return tensor / (1.0 + jnp.exp(-tensor))
-
-
-def matmul(left, right):
-    return jnp.dot(left, right, preferred_element_type=jnp.float32)
+B_N = 8
+A_N = 8
+HALF = 1024
+
+
+def mid_kernel(
+    part_ref, hid_ref, fg_ref, meta_ref, eg_ref, eu_ref, ed_ref, *rest,
+):
+    dw = rest[:8]
+    (out_ref, pbuf, metas, tok, p_s, pst_s, wg, wu, wdn, dws, disp, xin, ybuf, ysend, yrecv, zbuf, ret, dbuf, dsend,
+     drecv, rsend, rs, obuf, fres,
+     s_tp, r_tp, s_meta, r_meta, s_tok, r_tok, s_fwd, r_fwd, s_dis, r_dis, s_xf, r_xf, s_y, r_y, s_ret, r_ret, s_dn, r_dn,
+     s_rs, r_rs, s_out, r_out, l_w, l_d) = rest[8:]
+    ep = lax.axis_index("ep")
+    t = lax.axis_index("tp")
+    b = ep // 8
+    a = ep % 8
+    mate = (ep, 1 - t)
+
+    loads = [
+        pltpu.make_async_copy(eg_ref.at[0], wg, l_w.at[0]),
+        pltpu.make_async_copy(eu_ref.at[0], wu, l_w.at[1]),
+        pltpu.make_async_copy(ed_ref.at[0], wdn, l_w.at[2]),
+    ]
+    dloads = [pltpu.make_async_copy(dw[k], dws.at[k], l_d.at[k]) for k in range(8)]
+
+    def b_peer(k):
+        return ((b + k) % 8) * 8 + a
+
+    def a_peer(k):
+        return b * 8 + (a + k) % 8
+
+    barrier = pltpu.get_barrier_semaphore()
+    pl.semaphore_signal(barrier, inc=1, device_id=mate, device_id_type=MESH)
+    for k in range(1, 8):
+        pl.semaphore_signal(barrier, inc=1, device_id=(b_peer(k), t), device_id_type=MESH)
+        pl.semaphore_signal(barrier, inc=1, device_id=(a_peer(k), t), device_id_type=MESH)
+    for c in loads + dloads:
+        c.start()
+    pl.semaphore_wait(barrier, 15)
+
+    def send(src, dst, s, r, dev):
+        c = pltpu.make_async_remote_copy(
+            src_ref=src, dst_ref=dst, send_sem=s, recv_sem=r, device_id=dev, device_id_type=MESH
+        )
+        c.start()
+        return c
+
+    pending = []
+    c_tp = send(part_ref, pbuf, s_tp, r_tp, mate)
+    metas[b] = meta_ref[...]
+    c_meta = [send(meta_ref, metas.at[b], s_meta.at[k], r_meta.at[k], (b_peer(k), t)) for k in range(1, 8)]
+    c_tp.wait()
+    attn = part_ref[...].astype(jnp.float32) + pbuf[...].astype(jnp.float32)
+    first = (hid_ref[...].astype(jnp.float32) + attn).astype(jnp.bfloat16)
+    fres[0] = first[:, :HALF]
+    fres[1] = first[:, HALF:]
+    f32 = first.astype(jnp.float32)
+    ffn = (
+        f32 * lax.rsqrt(jnp.mean(f32 * f32, axis=-1, keepdims=True) + 1e-06) * fg_ref[...]
+    ).astype(jnp.bfloat16)
+    mine = pl.ds(pl.multiple_of(b * 64, 64), 64)
+    tok[0, mine, :] = ffn[:, :HALF]
+    tok[1, mine, :] = ffn[:, HALF:]
+    c_tok = [
+        send(tok.at[t, mine, :], tok.at[t, mine, :], s_tok.at[k], r_tok.at[k], (b_peer(k), t)) for k in range(1, 8)
+    ]
+
+    for c in c_meta:
+        c.wait()
+    low = lax.broadcasted_iota(jnp.int32, (8, 128), 1) < 64
+    rows = jnp.concatenate([jnp.where(low, metas[2 * i], metas[2 * i + 1]) for i in range(4)], axis=1)
+    ids = (lax.broadcasted_iota(jnp.int32, (8, 512), 0) + b * 8).astype(jnp.float32)
+    hit0, hit1 = rows[0:1] == ids, rows[1:2] == ids
+    one0, one1 = jnp.where(hit0, 1.0, 0.0), jnp.where(hit1, 1.0, 0.0)
+    hit = one0 + one1
+    scale = one0 * rows[2:3] + one1 * rows[3:4]
+    upper = jnp.where(
+        lax.broadcasted_iota(jnp.int32, (512, 512), 0) < lax.broadcasted_iota(jnp.int32, (512, 512), 1), 1.0, 0.0
+    ).astype(jnp.bfloat16)
+    rank = dot(hit.astype(jnp.bfloat16), upper)
+    rank = jnp.where(hit > 0.5, rank, -1.0)
+    place = lax.broadcasted_iota(jnp.int32, (32, 512), 0).astype(jnp.float32)
+    for j in range(8):
+        same = rank[j : j + 1] == place
+        p_s[pl.ds(j * 32, 32), :] = jnp.where(same, 1.0, 0.0).astype(jnp.bfloat16)
+    for i in range(2):
+        block = jnp.concatenate(
+            [
+                jnp.where(rank[j : j + 1] == place, jnp.broadcast_to(scale[j : j + 1], (32, 512)), 0.0)
+                for j in range(4 * i, 4 * i + 4)
+            ],
+            axis=0,
+        )
+        pst_s[:, i * 128 : (i + 1) * 128] = block.T.astype(jnp.bfloat16)
+
+    c_fwd = []
+    for k in range(1, 8):
+        c_tok[k - 1].wait()
+        his = pl.ds(pl.multiple_of(((b + 8 - k) % 8) * 64, 64), 64)
+        c_fwd.append(send(tok.at[t, his, :], tok.at[t, his, :], s_fwd.at[k], r_fwd.at[k], mate))
+
+    disp[...] = dot(p_s[...], tok[t]).astype(jnp.bfloat16).reshape(8, 32, HALF)
+    c_dis = [
+        send(disp.at[(a + k) % 8], xin.at[t, a], s_dis.at[k], r_dis.at[k], (a_peer(k), t)) for k in range(1, 8)
+    ]
+    xin[t, a] = disp[a]
+    c_xf = [send(disp.at[a], xin.at[t, a], s_xf.at[0], r_xf.at[0], mate)]
+
+    for c in c_fwd:
+        c.wait()
+    for c in dloads:
+        c.wait()
+    gate = dws[:, 0].reshape(384, 2048)
+    up = dws[:, 1].reshape(384, 2048)
+    down = dws[:, 2].reshape(384, 2048)
+    g = nt_dot(tok[0], gate[:, :HALF]) + nt_dot(tok[1], gate[:, HALF:])
+    u = nt_dot(tok[0], up[:, :HALF]) + nt_dot(tok[1], up[:, HALF:])
+    blend = 1.0 / (1.0 + jnp.exp(-g[:, 44:45]))
+    act = (g / (1.0 + jnp.exp(-g)) * u).astype(jnp.bfloat16)
+    dbuf[0] = dot(act, down[:, :HALF]) * blend
+    dbuf[1] = dot(act, down[:, HALF:]) * blend
+    dsend[...] = dbuf[1 - t].astype(jnp.bfloat16)
+    c_dn = send(dsend, drecv, s_dn, r_dn, mate)
+
+    for k in range(1, 8):
+        c_dis[k - 1].wait()
+        src = (a + 8 - k) % 8
+        c_xf.append(send(xin.at[t, src], xin.at[t, src], s_xf.at[k], r_xf.at[k], mate))
+    for c in loads:
+        c.wait()
+    for c in c_xf:
+        c.wait()
+    x0 = xin[0].reshape(256, HALF)
+    x1 = xin[1].reshape(256, HALF)
+    g = dot(x0, wg[:HALF]) + dot(x1, wg[HALF:])
+    u = dot(x0, wu[:HALF]) + dot(x1, wu[HALF:])
+    act = (g / (1.0 + jnp.exp(-g)) * u).astype(jnp.bfloat16)
+    ybuf[0] = dot(act, wdn[:, :HALF])
+    ybuf[1] = dot(act, wdn[:, HALF:])
+    ysend[...] = ybuf[1 - t].astype(jnp.bfloat16)
+    c_y = send(ysend, yrecv, s_y, r_y, mate)
+    c_y.wait()
+    zbuf[...] = (ybuf[t] + yrecv[...].astype(jnp.float32)).astype(jnp.bfloat16).reshape(8, 32, HALF)
+    c_ret = [
+        send(zbuf.at[(a + k) % 8], ret.at[a], s_ret.at[k], r_ret.at[k], (a_peer(k), t)) for k in range(1, 8)
+    ]
+    ret[a] = zbuf[a]
+    c_dn.wait()
+    for c in c_ret:
+        c.wait()
+    both = dot(pst_s[...], ret[...].reshape(256, HALF)) + dbuf[t] + drecv[...].astype(jnp.float32)
+    rsend[...] = both.astype(jnp.bfloat16).reshape(8, 64, HALF)
+    c_rs = [
+        send(rsend.at[(b + k) % 8], rs.at[b], s_rs.at[k], r_rs.at[k], (b_peer(k), t)) for k in range(1, 8)
+    ]
+    rs[b] = rsend[b]
+    for c in c_rs:
+        c.wait()
+    total = rs[0].astype(jnp.float32)
+    for i in range(1, 8):
+        total += rs[i].astype(jnp.float32)
+    obuf[t] = (fres[t].astype(jnp.float32) + total).astype(jnp.bfloat16)
+    c_out = send(obuf.at[t], obuf.at[t], s_out, r_out, mate)
+    c_out.wait()
+    out_ref[:, :HALF] = obuf[0]
+    out_ref[:, HALF:] = obuf[1]
+
+
+def middle(part, hidden, ffn_gain, meta, eg, eu, ed, dense):
+    vm = pl.BlockSpec(memory_space=pltpu.VMEM)
+    anyw = pl.BlockSpec(memory_space=pl.ANY)
+    bf, f4 = jnp.bfloat16, jnp.float32
+    dma = pltpu.SemaphoreType.DMA
+    scratch = [
+        pltpu.VMEM((64, 2048), bf),
+        pltpu.VMEM((8, 8, 128), f4),
+        pltpu.VMEM((2, 512, HALF), bf),
+        pltpu.VMEM((256, 512), bf),
+        pltpu.VMEM((512, 256), bf),
+        pltpu.VMEM((2048, 768), bf),
+        pltpu.VMEM((2048, 768), bf),
+        pltpu.VMEM((768, 2048), bf),
+        pltpu.VMEM((8, 3, 48, 2048), bf),
+        pltpu.VMEM((8, 32, HALF), bf),
+        pltpu.VMEM((2, 8, 32, HALF), bf),
+        pltpu.VMEM((2, 256, HALF), f4),
+        pltpu.VMEM((256, HALF), bf),
+        pltpu.VMEM((256, HALF), bf),
+        pltpu.VMEM((8, 32, HALF), bf),
+        pltpu.VMEM((8, 32, HALF), bf),
+        pltpu.VMEM((2, 512, HALF), f4),
+        pltpu.VMEM((512, HALF), bf),
+        pltpu.VMEM((512, HALF), bf),
+        pltpu.VMEM((8, 64, HALF), bf),
+        pltpu.VMEM((8, 64, HALF), bf),
+        pltpu.VMEM((2, 64, HALF), bf),
+        pltpu.VMEM((2, 64, HALF), bf),
+        dma, dma, dma((8,)), dma((8,)), dma((8,)), dma((8,)), dma((8,)), dma((8,)), dma((8,)), dma((8,)),
+        dma((8,)), dma((8,)), dma, dma, dma((8,)), dma((8,)), dma, dma, dma((8,)), dma((8,)), dma, dma,
+        dma((3,)), dma((8,)),
+    ]
+    return pl.pallas_call(
+        mid_kernel,
+        out_shape=jax.ShapeDtypeStruct(hidden.shape, bf),
+        in_specs=[vm] * 4 + [anyw] * 11,
+        out_specs=vm,
+        scratch_shapes=scratch,
+        compiler_params=pltpu.CompilerParams(
+            collective_id=0, has_side_effects=True, vmem_limit_bytes=62 * 1024 * 1024
+        ),
+        cost_estimate=pl.CostEstimate(flops=40_000_000_000, bytes_accessed=16_000_000, transcendentals=0),
+        name="middle",
+    )(part, hidden, ffn_gain.reshape(1, -1), meta, eg, eu, ed, *dense)
+
+
+def dense_shift(dx, dy):
+    pairs = []
+    for ep in range(64):
+        b, y, x = ep // 8, ep // 4 % 2, ep % 4
+        pairs.append((ep, b * 8 + (y + dy) % 2 * 4 + (x + dx) % 4))
+    return pairs
 
 
 def shards(
-    hidden,
-    mix_gain,
-    recept_weight,
-    key_weight,
-    value_weight,
-    decay_down,
-    decay_up,
-    decay_bias,
-    rate_down,
-    rate_up,
-    rate_bias,
-    head_gain,
-    out_weight,
-    memory_state,
-    ffn_gain,
-    blend_vector,
-    dense_gate,
-    dense_up,
-    dense_down,
-    expert_gate,
-    expert_up,
-    expert_down,
-    routing,
-    route_scale,
+    hidden, mix_gain, recept_weight, key_weight, value_weight, decay_down, decay_up, decay_bias, rate_down, rate_up,
+    rate_bias, head_gain, out_weight, memory_state, ffn_gain, blend_vector, dense_gate, dense_up, dense_down,
+    expert_gate, expert_up, expert_down, routing, route_scale,
 ):
-    seq_count, model_width = hidden.shape
+    units, model = dense_down.shape
+    gap = jnp.zeros((48 - units, model), jnp.bfloat16)
+    gate = jnp.concatenate([dense_gate.T, blend_vector[None], gap[1:]], axis=0)
+    up = jnp.concatenate([dense_up.T, gap], axis=0)
+    down = jnp.concatenate([dense_down, gap], axis=0)
+    own = jnp.stack([gate, up, down])
+    dense = [own]
+    for dy in range(2):
+        for dx in range(4):
+            if dx or dy:
+                dense.append(lax.ppermute(own, "ep", dense_shift(dx, dy)))
+    info = jnp.concatenate([routing.T.astype(jnp.float32), route_scale.T, jnp.zeros((4, 64), jnp.float32)], axis=0)
+    meta = jnp.concatenate([info, info], axis=1)
     new_state, part = attention(
         hidden, mix_gain, recept_weight, key_weight, value_weight, decay_down, decay_up, decay_bias,
         rate_down, rate_up, rate_bias, head_gain, out_weight, memory_state,
     )
-    attn_sum = of_everyone(part, "tp").astype(
-        jnp.float32
-    )
-    first_res = (hidden.astype(jnp.float32) + attn_sum).astype(jnp.bfloat16)
-    ffn_in = rms_scaled(first_res, ffn_gain).astype(jnp.bfloat16)
-    blend = jax.nn.sigmoid(jnp.dot(ffn_in, blend_vector, preferred_element_type=jnp.float32))
-    piece = lax.all_gather(ffn_in, "ep", axis=0, tiled=True)
-    dense_act = (silu_of(matmul(piece, dense_gate)) * matmul(piece, dense_up)).astype(jnp.bfloat16)
-    own_units = lax.all_to_all(dense_act, "ep", split_axis=0, concat_axis=1, tiled=True)
-    dense_out = matmul(own_units, lax.all_gather(dense_down, "ep", axis=0, tiled=True))
-    dest_count = lax.axis_size("ep")
-    top_count = routing.shape[1]
-    slot_cap = max(2, 2 * seq_count * top_count // dest_count)
-    flat_route = routing.reshape(-1)
-    one_hot = (flat_route[:, None] == jnp.arange(dest_count, dtype=jnp.int32)[None, :]).astype(
-        jnp.int32
-    )
-    running = jnp.cumsum(one_hot, axis=0)
-    rank = jnp.sum((running - 1) * one_hot, axis=1)
-    slot = flat_route * slot_cap + rank
-    select = (slot[None, :] == jnp.arange(dest_count * slot_cap, dtype=jnp.int32)[:, None]).astype(
-        jnp.bfloat16
-    )
-    pair_rows = jnp.repeat(ffn_in, top_count, axis=0)
-    outgoing = (
-        matmul(select, pair_rows).astype(jnp.bfloat16).reshape(dest_count, slot_cap, model_width)
-    )
-    arrived = lax.all_to_all(outgoing, "ep", split_axis=0, concat_axis=0, tiled=True)
-    src_count, slot_items, width_in = arrived.shape
-    flat_in = arrived.reshape(src_count * slot_items, width_in)
-    expert_act = (silu_of(matmul(flat_in, expert_gate[0])) * matmul(flat_in, expert_up[0])).astype(
-        jnp.bfloat16
-    )
-    result = matmul(expert_act, expert_down[0]).reshape(src_count, slot_items, width_in)
-    returned = lax.all_to_all(
-        result.astype(jnp.bfloat16), "ep", split_axis=0, concat_axis=0, tiled=True
-    ).astype(result.dtype)
-    per_pair = jnp.take(returned.reshape(dest_count * slot_cap, model_width), slot, axis=0)
-    expert_sum = jnp.sum(
-        per_pair.reshape(seq_count, top_count, model_width) * route_scale[:, :, None], axis=1
-    )
-    mixed = of_everyone(
-        (expert_sum + blend[:, None] * dense_out).astype(jnp.bfloat16), "tp"
-    ).astype(jnp.float32)
-    layer_out = (first_res.astype(jnp.float32) + mixed).astype(jnp.bfloat16)
+    layer_out = middle(part, hidden, ffn_gain, meta, expert_gate, expert_up, expert_down, dense)
     return (layer_out, new_state)
 
 

time: 297 us -> 159 us (0.54)
  waiting for transfers between devices: 129 us -> 17.2 us
  Pallas kernels: 27 us -> 94 us
  local copies, waits for them, and re-layouts: 51.8 us -> 4.56 us
  matrix products: 32 us -> 0 us
  starting transfers between devices: 24 us -> 40.2 us
  between operations: 14.3 us -> 0.77 us
  blocking collectives: 9.78 us -> 0 us
  other arithmetic: 7.19 us -> 1.87 us
    all_gather x2 -> x0, waiting for transfers between devices: 112 us -> none  [the longest x1 62.6 us: shards(): piece = lax.all_gather(ffn_in, 'ep', axis=0, tiled=True)]
    pallas_call x0 -> x1, Pallas kernels: none -> 67.2 us  [middle(): pl.pallas_call(mid_kernel, out_shape=jax.ShapeDtypeStruct(hidden.shape, b...]
    ppermute x0 -> x7, starting transfers between devices: none -> 40.2 us  [shards(): dense.append(lax.ppermute(own, 'ep', dense_shift(dx, dy)))]
    dot_general x8 -> x0, matrix products: 32 us -> none  [the longest x7 31.8 us: matmul(): return jnp.dot(left, right, preferred_element_type=jnp.float32)]
    all_to_all x3 -> x0, starting transfers between devices: 23.9 us -> none  [the longest x1 11.5 us: shards(): lax.all_to_all(outgoing, 'ep', split_axis=0, concat_axis=0, tiled=True)]
    unnamed x38 -> x17, local copies, waits for them, and re-layouts: 21.3 us -> 2.85 us
    ppermute x0 -> x7, waiting for transfers between devices: none -> 17.2 us  [shards(): dense.append(lax.ppermute(own, 'ep', dense_shift(dx, dy)))]
    all_to_all x3 -> x0, waiting for transfers between devices: 16.2 us -> none  [the longest x1 16.2 us: shards(): lax.all_to_all(outgoing, 'ep', split_axis=0, concat_axis=0, tiled=True)]
  transfers between devices with their start and end apart: 5 -> 7, of which waited for: 3 -> 1; matrix products, arithmetic and copies ran while one was open for 25% -> 0% of each run, Pallas kernels for 0% -> 17%
where the time goes in v2:
time: 159 us
  Pallas kernels  94 us (59%)
  starting transfers between devices  40.2 us (25%)
  waiting for transfers between devices  17.2 us (11%)
  local copies, waits for them, and re-layouts  4.56 us (3%)
  other arithmetic  1.87 us (1%)
    pallas_call x1, Pallas kernels, middle(): pl.pallas_call(mid_kernel, out_shape=jax.ShapeDtypeStruct(hidden.shape, b...  67.2 us
    ppermute x7, starting transfers between devices, shards(): dense.append(lax.ppermute(own, 'ep', dense_shift(dx, dy)))  40.2 us
    pallas_call x1, Pallas kernels, attention(): pl.pallas_call(att_kernel, grid=(seqs // SB,), in_specs=[whole(o.shape) f...  26.8 us
    ppermute x7, waiting for transfers between devices, shards(): dense.append(lax.ppermute(own, 'ep', dense_shift(dx, dy)))  17.2 us
  transfers between devices with their start and end apart: 7, of which 1 were waited for; matrix products, arithmetic and copies ran while one was open for 0% of the time, Pallas kernels for 17%

profile of v2, /device:TPU:1, one launch (start us, length us, event | category | flops | bytes accessed | tf_op | source)
XLA Modules:
  0.0 158.6 jit_solution(4195987932508064555)
XLA Ops:
  0.6 0.7 broadcast_in_dim.8
  1.3 0.9 pad_bitcast_fusion.1
  2.3 0.1 pad.7.clone
  2.4 1.1 maximum_bitcast_fusion
  3.5 0.1 pad_maximum_fusion.rest_0_
  3.6 0.0 copy-start
  3.6 4.4 %collective-permute-start.6 = (bf16[3,48,2048]{2,1,0:T(8,128)(2,1)S(1)}, bf16[3,48,2048]{2,1,0:T(8,128)(2,1)S(1)}, u32[]{:S(2)}, u32[]{:S(2)}) collective-permute-start(bf16[3,48,2048]{2,1,0:T(8,128)(2,1)S(1)} %pad_maximum_fusion.rest_0_), channel_id=1, source_target_pairs={{0,14},{2,8},{4,10},{6,12},{8,6},{10,0},{12,2},{14,4},{16,30},{18,... | collective-permute-start | bytes 1769480 | tf_op jit(solution)/shard_map/ppermute | solution.py:356
  7.9 0.4 collective-permute-start.5
  8.4 1.6 %collective-permute-start.4 = (bf16[3,48,2048]{2,1,0:T(8,128)(2,1)S(1)}, bf16[3,48,2048]{2,1,0:T(8,128)(2,1)S(1)}, u32[]{:S(2)}, u32[]{:S(2)}) collective-permute-start(bf16[3,48,2048]{2,1,0:T(8,128)(2,1)S(1)} %pad_maximum_fusion.rest_0_), channel_id=1, source_target_pairs={{0,10},{2,12},{4,14},{6,8},{8,2},{10,4},{12,6},{14,0},{16,26},{18,... | collective-permute-start | bytes 1769480 | tf_op jit(solution)/shard_map/ppermute | solution.py:356
  10.0 0.2 collective-permute-start.3
  10.1 2.1 %collective-permute-start.2 = (bf16[3,48,2048]{2,1,0:T(8,128)(2,1)S(1)}, bf16[3,48,2048]{2,1,0:T(8,128)(2,1)S(1)}, u32[]{:S(2)}, u32[]{:S(2)}) collective-permute-start(bf16[3,48,2048]{2,1,0:T(8,128)(2,1)S(1)} %pad_maximum_fusion.rest_0_), channel_id=1, source_target_pairs={{0,6},{2,0},{4,2},{6,4},{8,14},{10,8},{12,10},{14,12},{16,22},{18,... | collective-permute-start | bytes 1769480 | tf_op jit(solution)/shard_map/ppermute | solution.py:356
  12.2 17.2 %collective-permute-done.6.rest_7_ = bf16[3,48,2048]{2,1,0:T(8,128)(2,1)S(1)} collective-permute-done((bf16[3,48,2048]{2,1,0:T(8,128)(2,1)S(1)}, bf16[3,48,2048]{2,1,0:T(8,128)(2,1)S(1)}, u32[]{:S(2)}, u32[]{:S(2)}) %collective-permute-start.6) | collective-permute-done | bytes 589856 | tf_op jit(solution)/shard_map/ppermute | solution.py:356
  29.4 11.5 %collective-permute-start.1 = (bf16[3,48,2048]{2,1,0:T(8,128)(2,1)S(1)}, bf16[3,48,2048]{2,1,0:T(8,128)(2,1)}, u32[]{:S(2)}, u32[]{:S(2)}) collective-permute-start(bf16[3,48,2048]{2,1,0:T(8,128)(2,1)S(1)} %pad_maximum_fusion.rest_0_), channel_id=1, source_target_pairs={{0,4},{2,6},{4,0},{6,2},{8,12},{10,14},{12,8},{14,10},{16,20},{18,... | collective-permute-start | bytes 1769480 | tf_op jit(solution)/shard_map/ppermute | solution.py:356
  40.9 0.0 collective-permute-done.5.rest_6_
  41.0 20.0 %collective-permute-start = (bf16[3,48,2048]{2,1,0:T(8,128)(2,1)S(1)}, bf16[3,48,2048]{2,1,0:T(8,128)(2,1)}, u32[]{:S(2)}, u32[]{:S(2)}) collective-permute-start(bf16[3,48,2048]{2,1,0:T(8,128)(2,1)S(1)} %pad_maximum_fusion.rest_0_), channel_id=1, source_target_pairs={{0,2},{2,4},{4,6},{6,0},{8,10},{10,12},{12,14},{14,8},{16,18},{18,... | collective-permute-start | bytes 1769480 | tf_op jit(solution)/shard_map/ppermute | solution.py:356
  61.0 26.8 %attention.1 = (f32[64,8,64,64]{3,2,1,0:T(8,128)}, bf16[64,2048]{1,0:T(8,128)(2,1)}) custom-call(bf16[64,2048]{1,0:T(8,128)(2,1)} %hid_ref.3, f32[1,2048]{1,0:T(1,128)} %bitcast.23, bf16[2048,512]{1,0:T(8,128)(2,1)} %wr_ref.1, bf16[2048,512]{1,0:T(8,128)(2,1)} %wk_ref.1, bf16[2048,512]{1,0:T(8,128)(2,1)} %wv_ref.1, bf16[64,2048]{1,0:T(8,128)(2,1)} %bitcast.21, ...), custom_call_target="tpu_custom_call" | custom-call | flops 40000000000 | bytes 44000000 | tf_op jit(solution)/shard_map/attention/pallas_call | solution.py:98
  87.8 0.0 copy-done
  87.8 0.0 copy-done.3
  87.8 0.0 copy-done.4
  87.8 0.0 copy-done.1
  87.9 0.7 maximum_maximum_fusion.meta_ref
  88.6 0.0 collective-permute-done.4.rest_5_
  88.6 0.0 collective-permute-done.3.rest_4_
  88.6 0.0 copy-start.6
  88.6 0.0 collective-permute-done.2.rest_3_
  88.6 0.0 collective-permute-done.1.rest_2_
  88.6 0.0 collective-permute-done.rest_1_
  88.6 0.8 copy-done.5
  89.4 0.2 copy-done.6
  89.6 0.2 copy-done.7
  89.8 67.2 %middle.1 = bf16[64,2048]{1,0:T(8,128)(2,1)} custom-call(bf16[64,2048]{1,0:T(8,128)(2,1)} %get-tuple-element.4.part_ref, bf16[64,2048]{1,0:T(8,128)(2,1)} %hid_ref.3, f32[1,2048]{1,0:T(1,128)} %bitcast.24, f32[8,128]{1,0:T(8,128)} %maximum_maximum_fusion.meta_ref, bf16[1,2048,768]{2,1,0:T(8,128)(2,1)} %eg_ref.1, bf16[1,2048,768]{2,1,0:T(8,128)(2,1)} %eu_ref.1, ...), custom_call_target="tpu_custom_call" | custom-call | flops 40000000000 | bytes 16000000 | tf_op jit(solution)/shard_map/middle/pallas_call | solution.py:319
  157.0 1.7 %copy.27 = bf16[64,2048]{1,0:T(8,128)(2,1)} copy(bf16[64,2048]{1,0:T(8,128)(2,1)} %middle.1) | data formatting | bytes 524288
  (10 shorter events, 0.0 us)
Async XLA Ops:
  3.6 84.3 %copy-start = (bf16[3,48,2048]{2,1,0:T(8,128)(2,1)}, bf16[3,48,2048]{2,1,0:T(8,128)(2,1)S(1)}, u32[]{:S(2)}) copy-start(bf16[3,48,2048]{2,1,0:T(8,128)(2,1)S(1)} %pad_maximum_fusion.rest_0_) | copy-start | bytes 1769476
  3.6 25.9 %collective-permute-start.6 = (bf16[3,48,2048]{2,1,0:T(8,128)(2,1)S(1)}, bf16[3,48,2048]{2,1,0:T(8,128)(2,1)S(1)}, u32[]{:S(2)}, u32[]{:S(2)}) collective-permute-start(bf16[3,48,2048]{2,1,0:T(8,128)(2,1)S(1)} %pad_maximum_fusion.rest_0_), channel_id=1, source_target_pairs={{0,14},{2,8},{4,10},{6,12},{8,6},{10,0},{12,2},{14,4},{16,30},{18,... | collective-permute-start | bytes 1769480 | tf_op jit(solution)/shard_map/ppermute | solution.py:356
  7.9 33.0 %collective-permute-start.5 = (bf16[3,48,2048]{2,1,0:T(8,128)(2,1)S(1)}, bf16[3,48,2048]{2,1,0:T(8,128)(2,1)S(1)}, u32[]{:S(2)}, u32[]{:S(2)}) collective-permute-start(bf16[3,48,2048]{2,1,0:T(8,128)(2,1)S(1)} %pad_maximum_fusion.rest_0_), channel_id=1, source_target_pairs={{0,12},{2,14},{4,8},{6,10},{8,4},{10,6},{12,0},{14,2},{16,28},{18,... | collective-permute-start | bytes 1769480 | tf_op jit(solution)/shard_map/ppermute | solution.py:356
  8.4 80.2 %collective-permute-start.4 = (bf16[3,48,2048]{2,1,0:T(8,128)(2,1)S(1)}, bf16[3,48,2048]{2,1,0:T(8,128)(2,1)S(1)}, u32[]{:S(2)}, u32[]{:S(2)}) collective-permute-start(bf16[3,48,2048]{2,1,0:T(8,128)(2,1)S(1)} %pad_maximum_fusion.rest_0_), channel_id=1, source_target_pairs={{0,10},{2,12},{4,14},{6,8},{8,2},{10,4},{12,6},{14,0},{16,26},{18,... | collective-permute-start | bytes 1769480 | tf_op jit(solution)/shard_map/ppermute | solution.py:356
  10.0 78.6 %collective-permute-start.3 = (bf16[3,48,2048]{2,1,0:T(8,128)(2,1)S(1)}, bf16[3,48,2048]{2,1,0:T(8,128)(2,1)S(1)}, u32[]{:S(2)}, u32[]{:S(2)}) collective-permute-start(bf16[3,48,2048]{2,1,0:T(8,128)(2,1)S(1)} %pad_maximum_fusion.rest_0_), channel_id=1, source_target_pairs={{0,8},{2,10},{4,12},{6,14},{8,0},{10,2},{12,4},{14,6},{16,24},{18,... | collective-permute-start | bytes 1769480 | tf_op jit(solution)/shard_map/ppermute | solution.py:356
  10.1 78.4 %collective-permute-start.2 = (bf16[3,48,2048]{2,1,0:T(8,128)(2,1)S(1)}, bf16[3,48,2048]{2,1,0:T(8,128)(2,1)S(1)}, u32[]{:S(2)}, u32[]{:S(2)}) collective-permute-start(bf16[3,48,2048]{2,1,0:T(8,128)(2,1)S(1)} %pad_maximum_fusion.rest_0_), channel_id=1, source_target_pairs={{0,6},{2,0},{4,2},{6,4},{8,14},{10,8},{12,10},{14,12},{16,22},{18,... | collective-permute-start | bytes 1769480 | tf_op jit(solution)/shard_map/ppermute | solution.py:356
  29.4 58.4 %copy-start.3 = (bf16[3,48,2048]{2,1,0:T(8,128)(2,1)}, bf16[3,48,2048]{2,1,0:T(8,128)(2,1)S(1)}, u32[]{:S(2)}) copy-start(bf16[3,48,2048]{2,1,0:T(8,128)(2,1)S(1)} %collective-permute-done.6.rest_7_) | copy-start | bytes 1769476
  29.4 59.2 %collective-permute-start.1 = (bf16[3,48,2048]{2,1,0:T(8,128)(2,1)S(1)}, bf16[3,48,2048]{2,1,0:T(8,128)(2,1)}, u32[]{:S(2)}, u32[]{:S(2)}) collective-permute-start(bf16[3,48,2048]{2,1,0:T(8,128)(2,1)S(1)} %pad_maximum_fusion.rest_0_), channel_id=1, source_target_pairs={{0,4},{2,6},{4,0},{6,2},{8,12},{10,14},{12,8},{14,10},{16,20},{18,... | collective-permute-start | bytes 1769480 | tf_op jit(solution)/shard_map/ppermute | solution.py:356
  41.0 46.9 %copy-start.4 = (bf16[3,48,2048]{2,1,0:T(8,128)(2,1)}, bf16[3,48,2048]{2,1,0:T(8,128)(2,1)S(1)}, u32[]{:S(2)}) copy-start(bf16[3,48,2048]{2,1,0:T(8,128)(2,1)S(1)} %collective-permute-done.5.rest_6_) | copy-start | bytes 1769476
  41.0 47.7 %collective-permute-start = (bf16[3,48,2048]{2,1,0:T(8,128)(2,1)S(1)}, bf16[3,48,2048]{2,1,0:T(8,128)(2,1)}, u32[]{:S(2)}, u32[]{:S(2)}) collective-permute-start(bf16[3,48,2048]{2,1,0:T(8,128)(2,1)S(1)} %pad_maximum_fusion.rest_0_), channel_id=1, source_target_pairs={{0,2},{2,4},{4,6},{6,0},{8,10},{10,12},{12,14},{14,8},{16,18},{18,... | collective-permute-start | bytes 1769480 | tf_op jit(solution)/shard_map/ppermute | solution.py:356
  61.0 26.9 %copy-start.1 = (s32[64,2]{0,1:T(2,128)S(1)}, s32[64,2]{0,1:T(2,128)}, u32[]{:S(2)}) copy-start(s32[64,2]{0,1:T(2,128)} %param.46) | copy-start | bytes 1540
  61.0 26.9 %copy-start.2 = (f32[64,2]{0,1:T(2,128)S(1)}, f32[64,2]{0,1:T(2,128)}, u32[]{:S(2)}) copy-start(f32[64,2]{0,1:T(2,128)} %param.47) | copy-start | bytes 1540
  88.6 0.8 copy-start.5
  88.6 1.0 copy-start.6
  88.6 1.2 copy-start.7

commit v3 on v0

v3 whole, which is shorter than its diff:
```python
import jax
import jax.numpy as jnp
from jax import lax
from jax.experimental import pallas as pl
from jax.experimental.pallas import tpu as pltpu
from jax.sharding import PartitionSpec as P

MESH = pl.DeviceIdType.MESH
CH = 8
HALF = 1024


def dot(a, b):
    return jnp.dot(a, b, preferred_element_type=jnp.float32)


def nt_dot(a, b):
    return lax.dot_general(a, b, (((1,), (1,)), ((), ())), preferred_element_type=jnp.float32)


def iota(shape, dim):
    return lax.broadcasted_iota(jnp.int32, shape, dim)


def flag(cond, dtype=jnp.bfloat16):
    return jnp.where(cond, 1.0, 0.0).astype(dtype)


def layer_kernel(
    hid_ref, mixg_ref, dd_ref, du_ref, db_ref, rd_ref, ru_ref, rb_ref, hg_ref, fg_ref, bv_ref, dg_ref, dup_ref, ddn_ref,
    route_ref, scale_ref, wr_ref, wk_ref, wv_ref, ow_ref, st_ref, eg_ref, eu_ref, ed_ref,
    out_ref, k_s, d_s, l_s, v_s,
    wr, wk, wv, ow, st, g_s, bt_s, yt_s, part, pbuf, fres, tok, tq, pbig, pst, wg, wu, wdn, dws, disp, xin, xs, ybuf,
    ysend, yrecv, zsend, ret, dbuf, dsend, drecv, rsend, rs, obuf,
    l_a, l_s_sem, l_w, s_tp, r_tp, s_tok, r_tok, s_fwd, r_fwd, s_dis, r_dis, s_xf, r_xf, s_y, r_y, s_ret, r_ret,
    s_dn, r_dn, s_rs, r_rs, s_out, r_out, s_w, r_w,
):
    ep = lax.axis_index("ep")
    t = lax.axis_index("tp")
    b = ep // 8
    a = ep % 8
    x = ep % 4
    mate = (ep, 1 - t)
    ymate = (ep + 4 - 8 * ((ep // 4) % 2), t)
    xp = (ep - x + (x + 1) % 4, t)
    xm = (ep - x + (x + 3) % 4, t)
    heads, size = 8, 64
    width = heads * size

    def b_peer(k):
        return (((b + k) % 8) * 8 + a, t)

    barrier = pltpu.get_barrier_semaphore()
    pl.semaphore_signal(barrier, inc=1, device_id=mate, device_id_type=MESH)

    def greet(k, _):
        pl.semaphore_signal(barrier, inc=1, device_id=((ep + k) % 64, t), device_id_type=MESH)
        return 0

    lax.fori_loop(1, 64, greet, 0)

    aload = [
        pltpu.make_async_copy(src, dst, l_a.at[i])
        for i, (src, dst) in enumerate([(wk_ref, wk), (wr_ref, wr), (wv_ref, wv), (ow_ref, ow)])
    ]
    wload = [
        pltpu.make_async_copy(src.at[0], dst, l_w.at[i])
        for i, (src, dst) in enumerate([(eg_ref, wg), (eu_ref, wu), (ed_ref, wdn)])
    ]
    sload = [
        pltpu.make_async_copy(st_ref.at[pl.ds(c * CH, CH)], st.at[c % 4], l_s_sem.at[c]) for c in range(64 // CH)
    ]
    for c in aload[:3] + sload[:4] + aload[3:]:
        c.start()

    dws[0, :, 32:48, :] = jnp.zeros((3, 16, 2048), jnp.bfloat16)
    dws[0, 0, 0:44, :] = dg_ref[...]
    dws[0, 0, 44:45, :] = bv_ref[...]
    dws[0, 1, 0:44, :] = dup_ref[...]
    dws[0, 2, 0:44, :] = ddn_ref[...]

    def send(src, dst, s, r, dev):
        c = pltpu.make_async_remote_copy(
            src_ref=src, dst_ref=dst, send_sem=s, recv_sem=r, device_id=dev, device_id_type=MESH
        )
        c.start()
        return c

    pl.semaphore_wait(barrier, 64)
    first_half, second_half = pl.ds(0, HALF), pl.ds(HALF, HALF)
    w_y = send(dws.at[0], dws.at[1], s_w.at[0], r_w.at[0], ymate)
    w_xp = send(dws.at[0], dws.at[2], s_w.at[1], r_w.at[1], xp)
    w_xm = send(dws.at[0], dws.at[3], s_w.at[2], r_w.at[2], xm)

    own = pl.ds(pl.multiple_of(t * width, width), width)
    xh = hid_ref[...].astype(jnp.float32)
    nb = (xh * lax.rsqrt(jnp.mean(xh * xh, axis=-1, keepdims=True) + 1e-06) * mixg_ref[...]).astype(jnp.bfloat16)
    low = jnp.tanh(nt_dot(nb, dd_ref[...])).astype(jnp.bfloat16)
    pre = dot(low, du_ref[:, own]) + db_ref[:, own]
    dec = jnp.exp(-jnp.exp(-0.5) * (1.0 / (1.0 + jnp.exp(-pre))))
    rlow = nt_dot(nb, rd_ref[...]).astype(jnp.bfloat16)
    lr = 1.0 / (1.0 + jnp.exp(-(dot(rlow, ru_ref[:, own]) + rb_ref[:, own])))
    for c in aload[:3]:
        c.wait()
    key = dot(nb, wk[...]).astype(jnp.bfloat16).astype(jnp.float32)
    rec = dot(nb, wr[...]).astype(jnp.bfloat16).astype(jnp.float32)
    val = dot(nb, wv[...]).astype(jnp.bfloat16).astype(jnp.float32)
    for h in range(heads):
        cut = slice(h * size, (h + 1) * size)
        kh, lh, rh, vh = key[:, cut], lr[:, cut], rec[:, cut], val[:, cut]
        kn = kh * (1.0 / (jnp.sum(kh * kh, axis=-1, keepdims=True) + 1e-06))
        kl = kh * lh
        beta = jnp.sum(kl * rh, axis=-1, keepdims=True)
        k_s[h] = kn
        d_s[h] = dec[:, cut]
        l_s[h] = kl
        v_s[h] = vh
        g_s[h] = dec[:, cut] * rh - beta * kn
        bt_s[h] = beta * vh

    ids = iota((64, 64), 0).astype(jnp.float32)
    named = route_ref[...].astype(jnp.float32)
    one0, one1 = flag(named[0:1] == ids, jnp.float32), flag(named[1:2] == ids, jnp.float32)
    hit = one0 + one1
    scl = (one0 * scale_ref[0:1] + one1 * scale_ref[1:2]).astype(jnp.bfloat16)
    rank = dot(hit.astype(jnp.bfloat16), flag(iota((64, 64), 0) < iota((64, 64), 1)))
    rank = jnp.where(hit > 0.5, rank, -1.0).astype(jnp.bfloat16)
    tile = flag((iota((256, 64), 0) & 63) == iota((256, 64), 1))
    row, col = iota((1024, 256), 0), iota((1024, 256), 1)
    grown = dot(flag((iota((1024, 64), 0) >> 4) == iota((1024, 64), 1)), nt_dot(rank, tile).astype(jnp.bfloat16))
    pbig[...] = flag((grown == (row & 3).astype(jnp.float32)) & (((row >> 2) & 3) == (col >> 6)))
    row, col = iota((256, 1024), 0), iota((256, 1024), 1)
    spread = flag(iota((64, 1024), 0) == (iota((64, 1024), 1) >> 4))
    grown = dot(nt_dot(tile, rank).astype(jnp.bfloat16), spread)
    weight = dot(nt_dot(tile, scl).astype(jnp.bfloat16), spread)
    keep = (grown == (col & 3).astype(jnp.float32)) & (((col >> 2) & 3) == (row >> 6))
    pst[...] = jnp.where(keep, weight, 0.0).astype(jnp.bfloat16)

    lane = iota((size, 128), 1)
    chunks = 64 // CH
    w_2 = []
    for c in range(chunks):
        sload[c].wait()

        def one(j, _, c=c):
            for u in range(4):
                sl = j * 4 + u
                s = c * CH + sl
                for h in range(heads):
                    y = jnp.sum(st[c % 4, sl, h] * g_s[h, pl.ds(s, 1), :], axis=-1, keepdims=True)
                    yt_s[h] = jnp.where(lane == s, y, yt_s[h])
            return 0

        lax.fori_loop(0, CH // 4, one, 0)
        if c + 4 < chunks:
            sload[c + 4].start()
        if c == 3:
            for w in wload:
                w.start()
    for h in range(heads):
        y = yt_s[h].T[:64] + bt_s[h]
        cen = y - jnp.mean(y, axis=-1, keepdims=True)
        var = jnp.mean(cen * cen, axis=-1, keepdims=True)
        part[:, h * size : (h + 1) * size] = cen * lax.rsqrt(var + 0.00064)
    hn = (part[:, :width] * hg_ref[:, own]).astype(jnp.bfloat16)
    aload[3].wait()
    pbuf[0] = dot(hn, ow[...]).astype(jnp.bfloat16)
    c_tp = send(pbuf.at[0], pbuf.at[1], s_tp, r_tp, mate)
    w_y.wait()
    w_2.append(send(dws.at[1], dws.at[5], s_w.at[3], r_w.at[3], xp))
    w_2.append(send(dws.at[1], dws.at[6], s_w.at[4], r_w.at[4], xm))
    w_xp.wait()
    w_xm.wait()
    w_a = send(dws.at[2, :, :, first_half], dws.at[4, :, :, first_half], s_w.at[5], r_w.at[5], xp)
    w_b = send(dws.at[3, :, :, second_half], dws.at[4, :, :, second_half], s_w.at[6], r_w.at[6], xm)
    c_tp.wait()
    attn = pbuf[0].astype(jnp.float32) + pbuf[1].astype(jnp.float32)
    first = (hid_ref[...].astype(jnp.float32) + attn).astype(jnp.bfloat16)
    fres[0] = first[:, :HALF]
    fres[1] = first[:, HALF:]
    f32 = first.astype(jnp.float32)
    ffn = (
        f32 * lax.rsqrt(jnp.mean(f32 * f32, axis=-1, keepdims=True) + 1e-06) * fg_ref[...]
    ).astype(jnp.bfloat16)
    mine = pl.ds(pl.multiple_of(b * 64, 64), 64)
    tok[0, mine, :] = ffn[:, :HALF]
    tok[1, mine, :] = ffn[:, HALF:]
    c_tok = [send(tok.at[t, mine, :], tok.at[t, mine, :], s_tok.at[k], r_tok.at[k], b_peer(k)) for k in range(1, 8)]
    for q in range(8):
        tq[q // 4, (q % 4) * 64 : (q % 4 + 1) * 64, :] = ffn[:, q * 256 : (q + 1) * 256]
    disp[...] = dot(pbig[...], tq[t]).astype(jnp.bfloat16).reshape(64, 16, 256)

    def scatter(k, _):
        e = (ep + k) % 64
        send(disp.at[e], xin.at[t, ep], s_dis, r_dis, (e, t))
        return 0

    lax.fori_loop(1, 64, scatter, 0)
    xin[t, ep] = disp[ep]

    c_fwd = []
    for k in range(1, 8):
        c_tok[k - 1].wait()
        his = pl.ds(pl.multiple_of(((b + 8 - k) % 8) * 64, 64), 64)
        c_fwd.append(send(tok.at[t, his, :], tok.at[t, his, :], s_fwd.at[k], r_fwd.at[k], mate))
    most = pl.ds(0, 63)
    c_dis = pltpu.make_async_remote_copy(
        src_ref=disp.at[most], dst_ref=xin.at[t, most], send_sem=s_dis, recv_sem=r_dis, device_id=mate,
        device_id_type=MESH,
    )
    c_dis.wait()
    c_xf = send(xin.at[t], xin.at[t], s_xf, r_xf, mate)
    for w in w_2:
        w.wait()
    w_c = send(dws.at[5, :, :, first_half], dws.at[7, :, :, first_half], s_w.at[7], r_w.at[7], xp)
    w_d = send(dws.at[6, :, :, second_half], dws.at[7, :, :, second_half], s_w.at[8], r_w.at[8], xm)

    row, col = iota((256, 256), 0), iota((256, 256), 1)
    regroup = flag(
        (((row >> 6) == ((col >> 2) & 3)) & (((row >> 2) & 15) == (col >> 4))) & ((row & 3) == (col & 3))
    )
    ungroup = flag(
        (((col >> 6) == ((row >> 2) & 3)) & (((col >> 2) & 15) == (row >> 4))) & ((row & 3) == (col & 3))
    )
    c_xf.wait()
    for hf in range(2):
        for m in range(4):
            block = dot(regroup, xin[hf, m * 16 : (m + 1) * 16].reshape(256, 256)).astype(jnp.bfloat16)
            for q in range(4):
                xs[hf, m * 64 : (m + 1) * 64, q * 256 : (q + 1) * 256] = block[q * 64 : (q + 1) * 64]
    for w in wload:
        w.wait()
    g = dot(xs[0], wg[:HALF]) + dot(xs[1], wg[HALF:])
    u = dot(xs[0], wu[:HALF]) + dot(xs[1], wu[HALF:])
    act = (g / (1.0 + jnp.exp(-g)) * u).astype(jnp.bfloat16)
    ybuf[0] = dot(act, wdn[:, :HALF])
    ybuf[1] = dot(act, wdn[:, HALF:])
    ysend[...] = ybuf[1 - t].astype(jnp.bfloat16)
    c_y = send(ysend, yrecv, s_y, r_y, mate)
    c_y.wait()
    z = (ybuf[t] + yrecv[...].astype(jnp.float32)).astype(jnp.bfloat16)
    for m in range(4):
        block = jnp.concatenate([z[m * 64 : (m + 1) * 64, q * 256 : (q + 1) * 256] for q in range(4)], axis=0)
        zsend[m * 16 : (m + 1) * 16] = dot(ungroup, block).astype(jnp.bfloat16).reshape(16, 16, 256)

    def gather(k, _):
        e = (ep + k) % 64
        send(zsend.at[e], ret.at[ep], s_ret, r_ret, (e, t))
        return 0

    lax.fori_loop(1, 64, gather, 0)
    ret[ep] = zsend[ep]

    for c in c_fwd + [w_a, w_b, w_c, w_d]:
        c.wait()
    gate = dws[:, 0].reshape(384, 2048)
    up = dws[:, 1].reshape(384, 2048)
    down = dws[:, 2].reshape(384, 2048)
    g = nt_dot(tok[0], gate[:, :HALF]) + nt_dot(tok[1], gate[:, HALF:])
    u = nt_dot(tok[0], up[:, :HALF]) + nt_dot(tok[1], up[:, HALF:])
    blend = 1.0 / (1.0 + jnp.exp(-g[:, 44:45]))
    act = (g / (1.0 + jnp.exp(-g)) * u).astype(jnp.bfloat16)
    dbuf[0] = dot(act, down[:, :HALF]) * blend
    dbuf[1] = dot(act, down[:, HALF:]) * blend
    dsend[...] = dbuf[1 - t].astype(jnp.bfloat16)
    c_dn = send(dsend, drecv, s_dn, r_dn, mate)
    c_dn.wait()
    rsend[...] = (dbuf[t] + drecv[...].astype(jnp.float32)).astype(jnp.bfloat16).reshape(8, 64, HALF)
    c_rs = [send(rsend.at[(b + k) % 8], rs.at[b], s_rs.at[k], r_rs.at[k], b_peer(k)) for k in range(1, 8)]
    rs[b] = rsend[b]

    c_ret = pltpu.make_async_remote_copy(
        src_ref=zsend.at[most], dst_ref=ret.at[most], send_sem=s_ret, recv_sem=r_ret, device_id=mate,
        device_id_type=MESH,
    )
    c_ret.wait()
    comb = dot(pst[...], ret[...].reshape(1024, 256))
    for c in c_rs:
        c.wait()
    total = fres[t].astype(jnp.float32)
    for i in range(8):
        total += rs[i].astype(jnp.float32)
    for q in range(4):
        piece = slice(q * 256, (q + 1) * 256)
        obuf[t, :, piece] = (total[:, piece] + comb[q * 64 : (q + 1) * 64]).astype(jnp.bfloat16)
    c_out = send(obuf.at[t], obuf.at[t], s_out, r_out, mate)
    c_out.wait()
    out_ref[:, :HALF] = obuf[0]
    out_ref[:, HALF:] = obuf[1]


def layer(small, large):
    vm = pl.BlockSpec(memory_space=pltpu.VMEM)
    anyw = pl.BlockSpec(memory_space=pl.ANY)
    bf, f4 = jnp.bfloat16, jnp.float32
    dma = pltpu.SemaphoreType.DMA
    v = pltpu.VMEM
    scratch = [
        v((2048, 512), bf), v((2048, 512), bf), v((2048, 512), bf), v((512, 2048), bf),
        v((4, CH, 8, 64, 64), f4),
        v((8, 64, 64), f4), v((8, 64, 64), f4), v((8, 64, 128), f4),
        v((64, 512), f4), v((2, 64, 2048), bf), v((2, 64, HALF), bf),
        v((2, 512, HALF), bf), v((2, 256, 256), bf), v((1024, 256), bf), v((256, 1024), bf),
        v((2048, 768), bf), v((2048, 768), bf), v((768, 2048), bf),
        v((8, 3, 48, 2048), bf),
        v((64, 16, 256), bf), v((2, 64, 16, 256), bf), v((2, 256, HALF), bf),
        v((2, 256, HALF), f4), v((256, HALF), bf), v((256, HALF), bf),
        v((64, 16, 256), bf), v((64, 16, 256), bf),
        v((2, 512, HALF), f4), v((512, HALF), bf), v((512, HALF), bf),
        v((8, 64, HALF), bf), v((8, 64, HALF), bf), v((2, 64, HALF), bf),
        dma((4,)), dma((8,)), dma((3,)), dma, dma, dma((8,)), dma((8,)), dma((8,)), dma((8,)), dma, dma, dma, dma,
        dma, dma, dma, dma, dma, dma, dma((8,)), dma((8,)), dma, dma, dma((9,)), dma((9,)),
    ]
    rows = jax.ShapeDtypeStruct((8, 64, 64), f4)
    return pl.pallas_call(
        layer_kernel,
        out_shape=[jax.ShapeDtypeStruct((64, 2048), bf), rows, rows, rows, rows],
        in_specs=[vm] * len(small) + [anyw] * len(large),
        out_specs=[vm] * 5,
        scratch_shapes=scratch,
        compiler_params=pltpu.CompilerParams(
            collective_id=0, has_side_effects=True, vmem_limit_bytes=63 * 1024 * 1024
        ),
        name="layer",
    )(*small, *large)


SB = 8


def state_kernel(k_s, d_s, l_s, v_s, tokens_ref, st_ref, ns_ref, out_ref):
    step = pl.program_id(0)
    out_ref[...] = tokens_ref[...]
    eye = iota((64, 64), 0) == iota((64, 64), 1)

    def one(j, _):
        for u in range(2):
            sl = j * 2 + u
            row = pl.ds(step * SB + sl, 1)
            for h in range(8):
                m = st_ref[sl, h]
                w = jnp.sum(
                    jnp.where(eye, v_s[h, row, :], 0.0) - m * k_s[h, row, :], axis=-1, keepdims=True
                )
                ns_ref[sl, h] = m * d_s[h, row, :] + w * l_s[h, row, :]
        return 0

    lax.fori_loop(0, SB // 2, one, 0)


def new_states(k_s, d_s, l_s, v_s, tokens, state):
    fixed = pl.BlockSpec((8, 64, 64), lambda g: (0, 0, 0))
    blk = pl.BlockSpec((SB, 8, 64, 64), lambda g: (g, 0, 0, 0))
    slim = pl.BlockSpec((SB, 2048), lambda g: (g, 0))
    return pl.pallas_call(
        state_kernel,
        grid=(64 // SB,),
        in_specs=[fixed] * 4 + [slim, blk],
        out_specs=[blk, slim],
        out_shape=[
            jax.ShapeDtypeStruct(state.shape, jnp.float32),
            jax.ShapeDtypeStruct(tokens.shape, jnp.bfloat16),
        ],
        compiler_params=pltpu.CompilerParams(
            dimension_semantics=("arbitrary",), vmem_limit_bytes=40 * 1024 * 1024
        ),
        name="states",
    )(k_s, d_s, l_s, v_s, tokens, state)


def shards(
    hidden, mix_gain, recept_weight, key_weight, value_weight, decay_down, decay_up, decay_bias, rate_down, rate_up,
    rate_bias, head_gain, out_weight, memory_state, ffn_gain, blend_vector, dense_gate, dense_up, dense_down,
    expert_gate, expert_up, expert_down, routing, route_scale,
):
    flat = lambda vec: vec.reshape(1, -1)
    small = [
        hidden, flat(mix_gain), decay_down.T, decay_up, flat(decay_bias), rate_down.T, rate_up, flat(rate_bias),
        flat(head_gain), flat(ffn_gain), flat(blend_vector), dense_gate.T, dense_up.T, dense_down, routing.T,
        route_scale.T,
    ]
    large = [recept_weight, key_weight, value_weight, out_weight, memory_state, expert_gate, expert_up, expert_down]
    tokens, k_s, d_s, l_s, v_s = layer(small, large)
    new_state, layer_out = new_states(k_s, d_s, l_s, v_s, tokens, memory_state)
    return (layer_out, new_state)


def solution(mesh):
    in_specs = (
        P("ep", None),
        P(),
        P(None, "tp"),
        P(None, "tp"),
        P(None, "tp"),
        P(),
        P(),
        P(),
        P(),
        P(),
        P(),
        P(),
        P("tp", None),
        P("ep", "tp", None, None),
        P(),
        P(),
        P(None, ("ep", "tp")),
        P(None, ("ep", "tp")),
        P(("ep", "tp"), None),
        P("ep", None, "tp"),
        P("ep", None, "tp"),
        P("ep", "tp", None),
        P("ep", None),
        P("ep", None),
    )
    out_specs = (P("ep", None), P("ep", "tp", None, None))
    return jax.shard_map(shards, mesh=mesh, in_specs=in_specs, out_specs=out_specs, check_vma=False)
```

time: 325 us -> 109 us (0.34)
  waiting for transfers between devices: 141 us -> 0 us
  Pallas kernels: 0 us -> 102 us
  matrix products: 64.8 us -> 0 us
  local copies, waits for them, and re-layouts: 42.3 us -> 6.03 us
  other arithmetic: 27.9 us -> 0 us
  starting transfers between devices: 23.1 us -> 0 us
  between operations: 14.5 us -> 0.65 us
  blocking collectives: 9.79 us -> 0 us
    all_gather x2 -> x0, waiting for transfers between devices: 124 us -> none  [the longest x1 63.2 us: shards(): piece = lax.all_gather(ffn_in, 'ep', axis=0, tiled=True)]
    pallas_call x0 -> x2, Pallas kernels: none -> 102 us  [the longest x1 85 us: layer(): pl.pallas_call(layer_kernel, out_shape=[jax.ShapeDtypeStruct((64, 2048),...]
    dot_general x16 -> x0, matrix products: 64.8 us -> none  [the longest x13 43.4 us: matmul(): return jnp.dot(left, right, preferred_element_type=jnp.float32)]
    all_to_all x3 -> x0, starting transfers between devices: 23 us -> none  [the longest x1 11.7 us: shards(): lax.all_to_all(outgoing, 'ep', split_axis=0, concat_axis=0, tiled=True)]
    all_to_all x3 -> x0, waiting for transfers between devices: 16.2 us -> none  [the longest x1 16.2 us: shards(): lax.all_to_all(outgoing, 'ep', split_axis=0, concat_axis=0, tiled=True)]
    unnamed x52 -> x10, local copies, waits for them, and re-layouts: 19.6 us -> 4.74 us
    add x2 -> x0, other arithmetic: 13.7 us -> none  [the longest x1 13.7 us: shards(): memory_state * decay_rate[:, :, None, :]]
    all_to_all x2 -> x0, blocking collectives: 9.79 us -> none  [copy_for_each(): lax.all_to_all(jnp.broadcast_to(x[None], (length, *x.shape)), axis, 0, 0,...]
  transfers between devices with their start and end apart: 5 -> 0, of which waited for: 3 -> 0; matrix products, arithmetic and copies ran while one was open for 19% -> 0% of each run, Pallas kernels for 0% -> 0%
where the time goes in v3:
time: 109 us; the launch traced here: 108 us
  Pallas kernels  102 us (94%)
  local copies, waits for them, and re-layouts  6.03 us (6%)
    pallas_call x1, Pallas kernels, layer(): pl.pallas_call(layer_kernel, out_shape=[jax.ShapeDtypeStruct((64, 2048),...  85 us
    pallas_call x1, Pallas kernels, new_states(): pl.pallas_call(state_kernel, grid=(64 // SB,), in_specs=[fixed] * 4 + [sl...  16.8 us
    unnamed x10, local copies, waits for them, and re-layouts  4.74 us

profile of v3, /device:TPU:1, one launch (start us, length us, event | category | flops | bytes accessed | tf_op | source)
XLA Modules:
  0.0 108.4 jit_solution(18362289580496114917)
XLA Ops:
  0.6 1.3 %reshape.27.bv_ref = bf16[1,2048]{1,0:T(2,128)(2,1)} reshape(bf16[2048]{0:T(1024)(128)(2,1)} %param.39) | data formatting | bytes 8192 | tf_op jit(solution)/shard_map/reshape | solution.py:376
  1.9 85.0 %layer.1 = (bf16[64,2048]{1,0:T(8,128)(2,1)}, f32[8,64,64]{2,1,0:T(8,128)}, f32[8,64,64]{2,1,0:T(8,128)}, f32[8,64,64]{2,1,0:T(8,128)}, f32[8,64,64]{2,1,0:T(8,128)}) custom-call(bf16[64,2048]{1,0:T(8,128)(2,1)} %hid_ref.1, f32[1,2048]{1,0:T(1,128)} %bitcast.15, bf16[64,2048]{1,0:T(8,128)(2,1)} %bitcast.11, bf16[64,1024]{1,0:T(8,128)(2,1)} %du_ref.1, ...), custom_call_target="tpu_custom_call" | custom-call | tf_op jit(solution)/shard_map/layer/pallas_call | solution.py:315
  86.9 0.0 copy-start
  86.9 0.9 copy-done
  87.9 0.0 copy-start.1
  87.9 0.9 copy-done.1
  88.8 0.0 copy-start.2
  88.8 0.9 copy-done.2
  89.8 0.0 copy-start.3
  89.8 0.9 copy-done.3
  90.7 0.0 copy-start.4
  90.7 0.9 copy-done.4
  91.7 16.8 %states.1 = (f32[64,8,64,64]{3,2,1,0:T(8,128)}, bf16[64,2048]{1,0:T(8,128)(2,1)}) custom-call(f32[8,64,64]{2,1,0:T(8,128)S(1)} %copy-done.1, f32[8,64,64]{2,1,0:T(8,128)S(1)} %copy-done.2, f32[8,64,64]{2,1,0:T(8,128)S(1)} %copy-done.3, f32[8,64,64]{2,1,0:T(8,128)S(1)} %copy-done.4, bf16[64,2048]{1,0:T(8,128)(2,1)S(1)} %copy-done, f32[64,8,64,64]{3,2,1,0:T(8,128)} %st_ref.3), custom_call_target="tpu_custom_call" | custom-call | tf_op jit(solution)/shard_map/states/pallas_call | solution.py:355
Async XLA Ops:
  86.9 1.0 copy-start
  87.9 0.9 copy-start.1
  88.8 0.9 copy-start.2
  89.8 0.9 copy-start.3
  90.7 0.9 copy-start.4

commit v4 on v3

--- a/solution.py
+++ b/solution.py
@@ -27,29 +27,43 @@
 
 
 def layer_kernel(
-    hid_ref, mixg_ref, dd_ref, du_ref, db_ref, rd_ref, ru_ref, rb_ref, hg_ref, fg_ref, bv_ref, dg_ref, dup_ref, ddn_ref,
-    route_ref, scale_ref, wr_ref, wk_ref, wv_ref, ow_ref, st_ref, eg_ref, eu_ref, ed_ref,
-    out_ref, k_s, d_s, l_s, v_s,
-    wr, wk, wv, ow, st, g_s, bt_s, yt_s, part, pbuf, fres, tok, tq, pbig, pst, wg, wu, wdn, dws, disp, xin, xs, ybuf,
+    mixg_ref, db_ref, rb_ref, hg_ref, fg_ref, bv_ref, route_ref, scale_ref,
+    hid_in, dd_in, du_in, rd_in, ru_in, dg_in, dup_in, ddn_in, wr_ref, wk_ref, wv_ref, ow_ref, st_ref, eg_ref, eu_ref,
+    ed_ref,
+    out_ref, rows_ref,
+    hid_ref, dd_ref, du_ref, rd_ref, ru_ref, dg_ref, dup_ref, ddn_ref, wr, wk, wv, ow, st, g_s, bt_s, yt_s, part, pbuf, fres, tok, tq, pbig, pst, wg, wu, wdn, dws, disp, xin, xs, ybuf,
     ysend, yrecv, zsend, ret, dbuf, dsend, drecv, rsend, rs, obuf,
-    l_a, l_s_sem, l_w, s_tp, r_tp, s_tok, r_tok, s_fwd, r_fwd, s_dis, r_dis, s_xf, r_xf, s_y, r_y, s_ret, r_ret,
+    l_i, l_a, l_s_sem, l_w, s_tp, r_tp, s_tok, r_tok, s_fwd, r_fwd, s_dis, r_dis, s_xf, r_xf, s_y, r_y, s_ret, r_ret,
     s_dn, r_dn, s_rs, r_rs, s_out, r_out, s_w, r_w,
 ):
     ep = lax.axis_index("ep")
     t = lax.axis_index("tp")
-    b = ep // 8
-    a = ep % 8
-    x = ep % 4
+    place = (ep % 4, (ep // 4) % 4, ep // 16)
     mate = (ep, 1 - t)
-    ymate = (ep + 4 - 8 * ((ep // 4) % 2), t)
-    xp = (ep - x + (x + 1) % 4, t)
-    xm = (ep - x + (x + 3) % 4, t)
     heads, size = 8, 64
     width = heads * size
 
+    def chip(where):
+        return (where[2] * 16 + where[1] * 4 + where[0], t)
+
     def b_peer(k):
-        return (((b + k) % 8) * 8 + a, t)
-
+        return chip([(c + 2 * ((k >> d) & 1)) % 4 for d, c in enumerate(place)])
+
+    def beside(axis):
+        step = [0, 0, 0]
+        step[axis] = (1 - 2 * (place[axis] % 2)) * (1 - 2 * t) + 4
+        return chip([(c + o) % 4 for c, o in zip(place, step)])
+
+    k_s, d_s, l_s, v_s = rows_ref.at[0], rows_ref.at[1], rows_ref.at[2], rows_ref.at[3]
+    iload = [
+        pltpu.make_async_copy(src, dst, l_i.at[i])
+        for i, (src, dst) in enumerate([
+            (dg_in, dg_ref), (dup_in, dup_ref), (ddn_in, ddn_ref), (hid_in, hid_ref), (dd_in, dd_ref), (du_in, du_ref),
+            (rd_in, rd_ref), (ru_in, ru_ref),
+        ])
+    ]
+    for c in iload:
+        c.start()
     barrier = pltpu.get_barrier_semaphore()
     pl.semaphore_signal(barrier, inc=1, device_id=mate, device_id_type=MESH)
 
@@ -73,9 +87,12 @@
     for c in aload[:3] + sload[:4] + aload[3:]:
         c.start()
 
+    for c in iload:
+        c.wait()
     dws[0, :, 32:48, :] = jnp.zeros((3, 16, 2048), jnp.bfloat16)
     dws[0, 0, 0:44, :] = dg_ref[...]
-    dws[0, 0, 44:45, :] = bv_ref[...]
+    bv = bv_ref[...].astype(jnp.float32)
+    dws[0, 0, 44:45, :] = jnp.concatenate([bv[i : i + 1] for i in range(16)], axis=1).astype(jnp.bfloat16)
     dws[0, 1, 0:44, :] = dup_ref[...]
     dws[0, 2, 0:44, :] = ddn_ref[...]
 
@@ -87,10 +104,19 @@
         return c
 
     pl.semaphore_wait(barrier, 64)
-    first_half, second_half = pl.ds(0, HALF), pl.ds(HALF, HALF)
-    w_y = send(dws.at[0], dws.at[1], s_w.at[0], r_w.at[0], ymate)
-    w_xp = send(dws.at[0], dws.at[2], s_w.at[1], r_w.at[1], xp)
-    w_xm = send(dws.at[0], dws.at[3], s_w.at[2], r_w.at[2], xm)
+
+    def leg(n):
+        copies = []
+        for m in range(3):
+            axes = [(m + i) % 3 for i in range(3)]
+            for mask in range(1 << n):
+                held = sum(1 << axes[i] for i in range(n) if mask >> i & 1)
+                then = held + (1 << axes[n])
+                sem = m * 8 + then
+                copies.append(send(dws.at[held, m], dws.at[then, m], s_w.at[sem], r_w.at[sem], beside(axes[n])))
+        return copies
+
+    legs = leg(0)
 
     own = pl.ds(pl.multiple_of(t * width, width), width)
     xh = hid_ref[...].astype(jnp.float32)
@@ -136,9 +162,12 @@
     keep = (grown == (col & 3).astype(jnp.float32)) & (((col >> 2) & 3) == (row >> 6))
     pst[...] = jnp.where(keep, weight, 0.0).astype(jnp.bfloat16)
 
+    for w in legs:
+        w.wait()
+    legs = leg(1)
+
     lane = iota((size, 128), 1)
     chunks = 64 // CH
-    w_2 = []
     for c in range(chunks):
         sload[c].wait()
 
@@ -157,6 +186,10 @@
         if c == 3:
             for w in wload:
                 w.start()
+        if c == 5:
+            for w in legs:
+                w.wait()
+            legs = leg(2)
     for h in range(heads):
         y = yt_s[h].T[:64] + bt_s[h]
         cen = y - jnp.mean(y, axis=-1, keepdims=True)
@@ -166,13 +199,6 @@
     aload[3].wait()
     pbuf[0] = dot(hn, ow[...]).astype(jnp.bfloat16)
     c_tp = send(pbuf.at[0], pbuf.at[1], s_tp, r_tp, mate)
-    w_y.wait()
-    w_2.append(send(dws.at[1], dws.at[5], s_w.at[3], r_w.at[3], xp))
-    w_2.append(send(dws.at[1], dws.at[6], s_w.at[4], r_w.at[4], xm))
-    w_xp.wait()
-    w_xm.wait()
-    w_a = send(dws.at[2, :, :, first_half], dws.at[4, :, :, first_half], s_w.at[5], r_w.at[5], xp)
-    w_b = send(dws.at[3, :, :, second_half], dws.at[4, :, :, second_half], s_w.at[6], r_w.at[6], xm)
     c_tp.wait()
     attn = pbuf[0].astype(jnp.float32) + pbuf[1].astype(jnp.float32)
     first = (hid_ref[...].astype(jnp.float32) + attn).astype(jnp.bfloat16)
@@ -182,10 +208,8 @@
     ffn = (
         f32 * lax.rsqrt(jnp.mean(f32 * f32, axis=-1, keepdims=True) + 1e-06) * fg_ref[...]
     ).astype(jnp.bfloat16)
-    mine = pl.ds(pl.multiple_of(b * 64, 64), 64)
-    tok[0, mine, :] = ffn[:, :HALF]
-    tok[1, mine, :] = ffn[:, HALF:]
-    c_tok = [send(tok.at[t, mine, :], tok.at[t, mine, :], s_tok.at[k], r_tok.at[k], b_peer(k)) for k in range(1, 8)]
+    tok[0, 0:64, :] = ffn[:, :HALF]
+    tok[1, 0:64, :] = ffn[:, HALF:]
     for q in range(8):
         tq[q // 4, (q % 4) * 64 : (q % 4 + 1) * 64, :] = ffn[:, q * 256 : (q + 1) * 256]
     disp[...] = dot(pbig[...], tq[t]).astype(jnp.bfloat16).reshape(64, 16, 256)
@@ -197,12 +221,11 @@
 
     lax.fori_loop(1, 64, scatter, 0)
     xin[t, ep] = disp[ep]
-
-    c_fwd = []
-    for k in range(1, 8):
-        c_tok[k - 1].wait()
-        his = pl.ds(pl.multiple_of(((b + 8 - k) % 8) * 64, 64), 64)
-        c_fwd.append(send(tok.at[t, his, :], tok.at[t, his, :], s_fwd.at[k], r_fwd.at[k], mate))
+    c_tok = [
+        send(tok.at[t, pl.ds(0, 64), :], tok.at[t, pl.ds(k * 64, 64), :], s_tok.at[k], r_tok.at[k], b_peer(k))
+        for k in range(1, 8)
+    ]
+
     most = pl.ds(0, 63)
     c_dis = pltpu.make_async_remote_copy(
         src_ref=disp.at[most], dst_ref=xin.at[t, most], send_sem=s_dis, recv_sem=r_dis, device_id=mate,
@@ -210,11 +233,6 @@
     )
     c_dis.wait()
     c_xf = send(xin.at[t], xin.at[t], s_xf, r_xf, mate)
-    for w in w_2:
-        w.wait()
-    w_c = send(dws.at[5, :, :, first_half], dws.at[7, :, :, first_half], s_w.at[7], r_w.at[7], xp)
-    w_d = send(dws.at[6, :, :, second_half], dws.at[7, :, :, second_half], s_w.at[8], r_w.at[8], xm)
-
     row, col = iota((256, 256), 0), iota((256, 256), 1)
     regroup = flag(
         (((row >> 6) == ((col >> 2) & 3)) & (((row >> 2) & 15) == (col >> 4))) & ((row & 3) == (col & 3))
@@ -237,6 +255,12 @@
     ybuf[1] = dot(act, wdn[:, HALF:])
     ysend[...] = ybuf[1 - t].astype(jnp.bfloat16)
     c_y = send(ysend, yrecv, s_y, r_y, mate)
+    c_fwd = []
+    for k in range(1, 8):
+        c_tok[k - 1].wait()
+        his = pl.ds(k * 64, 64)
+        c_fwd.append(send(tok.at[t, his, :], tok.at[t, his, :], s_fwd.at[k], r_fwd.at[k], mate))
+
     c_y.wait()
     z = (ybuf[t] + yrecv[...].astype(jnp.float32)).astype(jnp.bfloat16)
     for m in range(4):
@@ -251,23 +275,32 @@
     lax.fori_loop(1, 64, gather, 0)
     ret[ep] = zsend[ep]
 
-    for c in c_fwd + [w_a, w_b, w_c, w_d]:
+    for c in legs + c_fwd:
         c.wait()
     gate = dws[:, 0].reshape(384, 2048)
     up = dws[:, 1].reshape(384, 2048)
     down = dws[:, 2].reshape(384, 2048)
-    g = nt_dot(tok[0], gate[:, :HALF]) + nt_dot(tok[1], gate[:, HALF:])
-    u = nt_dot(tok[0], up[:, :HALF]) + nt_dot(tok[1], up[:, HALF:])
-    blend = 1.0 / (1.0 + jnp.exp(-g[:, 44:45]))
-    act = (g / (1.0 + jnp.exp(-g)) * u).astype(jnp.bfloat16)
-    dbuf[0] = dot(act, down[:, :HALF]) * blend
-    dbuf[1] = dot(act, down[:, HALF:]) * blend
-    dsend[...] = dbuf[1 - t].astype(jnp.bfloat16)
-    c_dn = send(dsend, drecv, s_dn, r_dn, mate)
-    c_dn.wait()
-    rsend[...] = (dbuf[t] + drecv[...].astype(jnp.float32)).astype(jnp.bfloat16).reshape(8, 64, HALF)
-    c_rs = [send(rsend.at[(b + k) % 8], rs.at[b], s_rs.at[k], r_rs.at[k], b_peer(k)) for k in range(1, 8)]
-    rs[b] = rsend[b]
+    c_dn = []
+    for p in range(2):
+        part_rows = slice(p * 256, p * 256 + 256)
+        t0, t1 = tok[0, part_rows, :], tok[1, part_rows, :]
+        g = nt_dot(t0, gate[:, :HALF]) + nt_dot(t1, gate[:, HALF:])
+        u = nt_dot(t0, up[:, :HALF]) + nt_dot(t1, up[:, HALF:])
+        blend = 1.0 / (1.0 + jnp.exp(-g[:, 44:45]))
+        act = (g / (1.0 + jnp.exp(-g)) * u).astype(jnp.bfloat16)
+        dbuf[p, 0] = dot(act, down[:, :HALF]) * blend
+        dbuf[p, 1] = dot(act, down[:, HALF:]) * blend
+        dsend[p] = dbuf[p, 1 - t].astype(jnp.bfloat16)
+        c_dn.append(send(dsend.at[p], drecv.at[p], s_dn.at[p], r_dn.at[p], mate))
+    c_rs = []
+    for p in range(2):
+        c_dn[p].wait()
+        rsend[p * 4 : p * 4 + 4] = (
+            (dbuf[p, t] + drecv[p].astype(jnp.float32)).astype(jnp.bfloat16).reshape(4, 64, HALF)
+        )
+        for k in range(p * 4, p * 4 + 4):
+            if k:
+                c_rs.append(send(rsend.at[k], rs.at[k], s_rs.at[k], r_rs.at[k], b_peer(k)))
 
     c_ret = pltpu.make_async_remote_copy(
         src_ref=zsend.at[most], dst_ref=ret.at[most], send_sem=s_ret, recv_sem=r_ret, device_id=mate,
@@ -277,8 +310,8 @@
     comb = dot(pst[...], ret[...].reshape(1024, 256))
     for c in c_rs:
         c.wait()
-    total = fres[t].astype(jnp.float32)
-    for i in range(8):
+    total = fres[t].astype(jnp.float32) + rsend[0].astype(jnp.float32)
+    for i in range(1, 8):
         total += rs[i].astype(jnp.float32)
     for q in range(4):
         piece = slice(q * 256, (q + 1) * 256)
@@ -295,7 +328,7 @@
     bf, f4 = jnp.bfloat16, jnp.float32
     dma = pltpu.SemaphoreType.DMA
     v = pltpu.VMEM
-    scratch = [
+    scratch = [v(ref.shape, bf) for ref in large[:8]] + [
         v((2048, 512), bf), v((2048, 512), bf), v((2048, 512), bf), v((512, 2048), bf),
         v((4, CH, 8, 64, 64), f4),
         v((8, 64, 64), f4), v((8, 64, 64), f4), v((8, 64, 128), f4),
@@ -306,17 +339,16 @@
         v((64, 16, 256), bf), v((2, 64, 16, 256), bf), v((2, 256, HALF), bf),
         v((2, 256, HALF), f4), v((256, HALF), bf), v((256, HALF), bf),
         v((64, 16, 256), bf), v((64, 16, 256), bf),
-        v((2, 512, HALF), f4), v((512, HALF), bf), v((512, HALF), bf),
+        v((2, 2, 256, HALF), f4), v((2, 256, HALF), bf), v((2, 256, HALF), bf),
         v((8, 64, HALF), bf), v((8, 64, HALF), bf), v((2, 64, HALF), bf),
-        dma((4,)), dma((8,)), dma((3,)), dma, dma, dma((8,)), dma((8,)), dma((8,)), dma((8,)), dma, dma, dma, dma,
-        dma, dma, dma, dma, dma, dma, dma((8,)), dma((8,)), dma, dma, dma((9,)), dma((9,)),
-    ]
-    rows = jax.ShapeDtypeStruct((8, 64, 64), f4)
+        dma((8,)), dma((4,)), dma((8,)), dma((3,)), dma, dma, dma((8,)), dma((8,)), dma((8,)), dma((8,)), dma, dma, dma,
+        dma, dma, dma, dma, dma, dma((2,)), dma((2,)), dma((8,)), dma((8,)), dma, dma, dma((24,)), dma((24,)),
+    ]
     return pl.pallas_call(
         layer_kernel,
-        out_shape=[jax.ShapeDtypeStruct((64, 2048), bf), rows, rows, rows, rows],
+        out_shape=[jax.ShapeDtypeStruct((64, 2048), bf), jax.ShapeDtypeStruct((4, 8, 64, 64), f4)],
         in_specs=[vm] * len(small) + [anyw] * len(large),
-        out_specs=[vm] * 5,
+        out_specs=[vm] * 2,
         scratch_shapes=scratch,
         compiler_params=pltpu.CompilerParams(
             collective_id=0, has_side_effects=True, vmem_limit_bytes=63 * 1024 * 1024
@@ -325,47 +357,68 @@
     )(*small, *large)
 
 
-SB = 8
-
-
-def state_kernel(k_s, d_s, l_s, v_s, tokens_ref, st_ref, ns_ref, out_ref):
-    step = pl.program_id(0)
+SB = 4
+
+
+def state_kernel(rows_ref, tokens_ref, st_ref, ns_ref, out_ref, old, new, l_in, l_out):
+    count = st_ref.shape[0] // SB
+
+    def load(c):
+        own = pl.ds(c * SB, SB)
+        return pltpu.make_async_copy(st_ref.at[own], old.at[own], l_in.at[c])
+
+    def store(c):
+        own = pl.ds(c * SB, SB)
+        return pltpu.make_async_copy(new.at[own], ns_ref.at[own], l_out.at[c])
+
+    for c in range(count):
+        load(c).start()
     out_ref[...] = tokens_ref[...]
     eye = iota((64, 64), 0) == iota((64, 64), 1)
 
-    def one(j, _):
-        for u in range(2):
-            sl = j * 2 + u
-            row = pl.ds(step * SB + sl, 1)
+    def one(c, _):
+        load(c).wait()
+        for u in range(SB):
+            s = c * SB + u
+            row = pl.ds(s, 1)
             for h in range(8):
-                m = st_ref[sl, h]
+                m = old[s, h]
                 w = jnp.sum(
-                    jnp.where(eye, v_s[h, row, :], 0.0) - m * k_s[h, row, :], axis=-1, keepdims=True
+                    jnp.where(eye, rows_ref[3, h, row, :], 0.0) - m * rows_ref[0, h, row, :], axis=-1, keepdims=True
                 )
-                ns_ref[sl, h] = m * d_s[h, row, :] + w * l_s[h, row, :]
+                new[s, h] = m * rows_ref[1, h, row, :] + w * rows_ref[2, h, row, :]
+        store(c).start()
         return 0
 
-    lax.fori_loop(0, SB // 2, one, 0)
-
-
-def new_states(k_s, d_s, l_s, v_s, tokens, state):
-    fixed = pl.BlockSpec((8, 64, 64), lambda g: (0, 0, 0))
-    blk = pl.BlockSpec((SB, 8, 64, 64), lambda g: (g, 0, 0, 0))
-    slim = pl.BlockSpec((SB, 2048), lambda g: (g, 0))
+    lax.fori_loop(0, count, one, 0)
+
+    def drain(c, _):
+        store(c).wait()
+        return 0
+
+    lax.fori_loop(0, count, drain, 0)
+
+
+def new_states(rows, tokens, state):
+    vm = pl.BlockSpec(memory_space=pltpu.VMEM)
+    anyw = pl.BlockSpec(memory_space=pl.ANY)
     return pl.pallas_call(
         state_kernel,
-        grid=(64 // SB,),
-        in_specs=[fixed] * 4 + [slim, blk],
-        out_specs=[blk, slim],
+        in_specs=[vm, vm, anyw],
+        out_specs=[anyw, vm],
         out_shape=[
             jax.ShapeDtypeStruct(state.shape, jnp.float32),
             jax.ShapeDtypeStruct(tokens.shape, jnp.bfloat16),
         ],
-        compiler_params=pltpu.CompilerParams(
-            dimension_semantics=("arbitrary",), vmem_limit_bytes=40 * 1024 * 1024
-        ),
+        scratch_shapes=[
+            pltpu.VMEM(state.shape, jnp.float32),
+            pltpu.VMEM(state.shape, jnp.float32),
+            pltpu.SemaphoreType.DMA((state.shape[0] // SB,)),
+            pltpu.SemaphoreType.DMA((state.shape[0] // SB,)),
+        ],
+        compiler_params=pltpu.CompilerParams(vmem_limit_bytes=63 * 1024 * 1024),
         name="states",
-    )(k_s, d_s, l_s, v_s, tokens, state)
+    )(rows, tokens, state)
 
 
 def shards(
@@ -375,13 +428,15 @@
 ):
     flat = lambda vec: vec.reshape(1, -1)
     small = [
-        hidden, flat(mix_gain), decay_down.T, decay_up, flat(decay_bias), rate_down.T, rate_up, flat(rate_bias),
-        flat(head_gain), flat(ffn_gain), flat(blend_vector), dense_gate.T, dense_up.T, dense_down, routing.T,
-        route_scale.T,
-    ]
-    large = [recept_weight, key_weight, value_weight, out_weight, memory_state, expert_gate, expert_up, expert_down]
-    tokens, k_s, d_s, l_s, v_s = layer(small, large)
-    new_state, layer_out = new_states(k_s, d_s, l_s, v_s, tokens, memory_state)
+        flat(mix_gain), flat(decay_bias), flat(rate_bias), flat(head_gain), flat(ffn_gain), blend_vector.reshape(16, 128),
+        routing.T, route_scale.T,
+    ]
+    large = [
+        hidden, decay_down.T, decay_up, rate_down.T, rate_up, dense_gate.T, dense_up.T, dense_down,
+        recept_weight, key_weight, value_weight, out_weight, memory_state, expert_gate, expert_up, expert_down,
+    ]
+    tokens, rows = layer(small, large)
+    new_state, layer_out = new_states(rows, tokens, memory_state)
     return (layer_out, new_state)
 
 

time: 109 us -> 94.2 us (0.86)
  Pallas kernels: 102 us -> 93.2 us
  local copies, waits for them, and re-layouts: 6.03 us -> 0 us
    pallas_call x1, Pallas kernels: 85 us -> 79.2 us  [layer(): pl.pallas_call(layer_kernel, out_shape=[jax.ShapeDtypeStruct((64, 2048),...]
    unnamed x10 -> x0, local copies, waits for them, and re-layouts: 4.74 us -> none
    pallas_call x1, Pallas kernels: 16.8 us -> 13.9 us  [new_states(): pl.pallas_call(state_kernel, in_specs=[vm, vm, anyw], out_specs=[anyw, vm...]
    reshape x1 -> x0, local copies, waits for them, and re-layouts: 1.29 us -> none  [shards(): flat = lambda vec: vec.reshape(1, -1)]
where the time goes in v4:
time: 94.2 us; the launch traced here: 94 us
  Pallas kernels  93.2 us (99%)
    pallas_call x1, Pallas kernels, layer(): pl.pallas_call(layer_kernel, out_shape=[jax.ShapeDtypeStruct((64, 2048),...  79.2 us
    pallas_call x1, Pallas kernels, new_states(): pl.pallas_call(state_kernel, in_specs=[vm, vm, anyw], out_specs=[anyw, vm...  13.9 us

profile of v4, /device:TPU:1, one launch (start us, length us, event | category | flops | bytes accessed | tf_op | source)
XLA Modules:
  0.0 94.0 jit_solution(17180452651472780552)
XLA Ops:
  0.6 79.2 %layer.1 = (bf16[64,2048]{1,0:T(8,128)(2,1)}, f32[4,8,64,64]{3,2,1,0:T(8,128)}) custom-call(f32[1,2048]{1,0:T(1,128)} %bitcast.16, f32[1,1024]{1,0:T(1,128)} %bitcast.18, f32[1,1024]{1,0:T(1,128)} %bitcast.19, f32[1,1024]{1,0:T(1,128)} %bitcast.20, f32[1,2048]{1,0:T(1,128)} %bitcast.17, bf16[16,128]{1,0:T(8,128)(2,1)} %bitcast.21, s32[2,64]{1,0:T(2,128)} %bitcast.22, ...), custom_call_target="tpu_custom_call" | custom-call | tf_op jit(solution)/shard_map/layer/pallas_call | solution.py:347
  79.9 13.9 %states.1 = (f32[64,8,64,64]{3,2,1,0:T(8,128)}, bf16[64,2048]{1,0:T(8,128)(2,1)}) custom-call(f32[4,8,64,64]{3,2,1,0:T(8,128)} %get-tuple-element.6.rows_ref, bf16[64,2048]{1,0:T(8,128)(2,1)} %get-tuple-element.7.tokens_ref, f32[64,8,64,64]{3,2,1,0:T(8,128)} %st_ref.3), custom_call_target="tpu_custom_call" | custom-call | tf_op jit(solution)/shard_map/states/pallas_call | solution.py:405

commit v5 on v4

--- a/solution.py
+++ b/solution.py
@@ -30,10 +30,10 @@
     mixg_ref, db_ref, rb_ref, hg_ref, fg_ref, bv_ref, route_ref, scale_ref,
     hid_in, dd_in, du_in, rd_in, ru_in, dg_in, dup_in, ddn_in, wr_ref, wk_ref, wv_ref, ow_ref, st_ref, eg_ref, eu_ref,
     ed_ref,
-    out_ref, rows_ref,
-    hid_ref, dd_ref, du_ref, rd_ref, ru_ref, dg_ref, dup_ref, ddn_ref, wr, wk, wv, ow, st, g_s, bt_s, yt_s, part, pbuf, fres, tok, tq, pbig, pst, wg, wu, wdn, dws, disp, xin, xs, ybuf,
-    ysend, yrecv, zsend, ret, dbuf, dsend, drecv, rsend, rs, obuf,
-    l_i, l_a, l_s_sem, l_w, s_tp, r_tp, s_tok, r_tok, s_fwd, r_fwd, s_dis, r_dis, s_xf, r_xf, s_y, r_y, s_ret, r_ret,
+    out_ref, ns_ref,
+    rows_ref, nsb, hid_ref, dd_ref, du_ref, rd_ref, ru_ref, dg_ref, dup_ref, ddn_ref, wr, wk, wv, ow, st, g_s, bt_s, yt_s, part, pbuf, fres, tok, tq, pbig, pst, wg, wu, wdn, dws, disp, xin, xs, ybuf,
+    ysend, yrecv, zsend, ret, dbuf, dsend, drecv, rsend, rs, rs2, obuf,
+    l_i, l_again, l_ns, l_a, l_s_sem, l_w, s_tp, r_tp, s_tok, r_tok, s_fwd, r_fwd, s_dis, r_dis, s_xf, r_xf, s_y, r_y, s_ret, r_ret,
     s_dn, r_dn, s_rs, r_rs, s_out, r_out, s_w, r_w,
 ):
     ep = lax.axis_index("ep")
@@ -86,63 +86,6 @@
     ]
     for c in aload[:3] + sload[:4] + aload[3:]:
         c.start()
-
-    for c in iload:
-        c.wait()
-    dws[0, :, 32:48, :] = jnp.zeros((3, 16, 2048), jnp.bfloat16)
-    dws[0, 0, 0:44, :] = dg_ref[...]
-    bv = bv_ref[...].astype(jnp.float32)
-    dws[0, 0, 44:45, :] = jnp.concatenate([bv[i : i + 1] for i in range(16)], axis=1).astype(jnp.bfloat16)
-    dws[0, 1, 0:44, :] = dup_ref[...]
-    dws[0, 2, 0:44, :] = ddn_ref[...]
-
-    def send(src, dst, s, r, dev):
-        c = pltpu.make_async_remote_copy(
-            src_ref=src, dst_ref=dst, send_sem=s, recv_sem=r, device_id=dev, device_id_type=MESH
-        )
-        c.start()
-        return c
-
-    pl.semaphore_wait(barrier, 64)
-
-    def leg(n):
-        copies = []
-        for m in range(3):
-            axes = [(m + i) % 3 for i in range(3)]
-            for mask in range(1 << n):
-                held = sum(1 << axes[i] for i in range(n) if mask >> i & 1)
-                then = held + (1 << axes[n])
-                sem = m * 8 + then
-                copies.append(send(dws.at[held, m], dws.at[then, m], s_w.at[sem], r_w.at[sem], beside(axes[n])))
-        return copies
-
-    legs = leg(0)
-
-    own = pl.ds(pl.multiple_of(t * width, width), width)
-    xh = hid_ref[...].astype(jnp.float32)
-    nb = (xh * lax.rsqrt(jnp.mean(xh * xh, axis=-1, keepdims=True) + 1e-06) * mixg_ref[...]).astype(jnp.bfloat16)
-    low = jnp.tanh(nt_dot(nb, dd_ref[...])).astype(jnp.bfloat16)
-    pre = dot(low, du_ref[:, own]) + db_ref[:, own]
-    dec = jnp.exp(-jnp.exp(-0.5) * (1.0 / (1.0 + jnp.exp(-pre))))
-    rlow = nt_dot(nb, rd_ref[...]).astype(jnp.bfloat16)
-    lr = 1.0 / (1.0 + jnp.exp(-(dot(rlow, ru_ref[:, own]) + rb_ref[:, own])))
-    for c in aload[:3]:
-        c.wait()
-    key = dot(nb, wk[...]).astype(jnp.bfloat16).astype(jnp.float32)
-    rec = dot(nb, wr[...]).astype(jnp.bfloat16).astype(jnp.float32)
-    val = dot(nb, wv[...]).astype(jnp.bfloat16).astype(jnp.float32)
-    for h in range(heads):
-        cut = slice(h * size, (h + 1) * size)
-        kh, lh, rh, vh = key[:, cut], lr[:, cut], rec[:, cut], val[:, cut]
-        kn = kh * (1.0 / (jnp.sum(kh * kh, axis=-1, keepdims=True) + 1e-06))
-        kl = kh * lh
-        beta = jnp.sum(kl * rh, axis=-1, keepdims=True)
-        k_s[h] = kn
-        d_s[h] = dec[:, cut]
-        l_s[h] = kl
-        v_s[h] = vh
-        g_s[h] = dec[:, cut] * rh - beta * kn
-        bt_s[h] = beta * vh
 
     ids = iota((64, 64), 0).astype(jnp.float32)
     named = route_ref[...].astype(jnp.float32)
@@ -162,9 +105,68 @@
     keep = (grown == (col & 3).astype(jnp.float32)) & (((col >> 2) & 3) == (row >> 6))
     pst[...] = jnp.where(keep, weight, 0.0).astype(jnp.bfloat16)
 
-    for w in legs:
+    for c in iload:
+        c.wait()
+    dws[0, :, 32:48, :] = jnp.zeros((3, 16, 2048), jnp.bfloat16)
+    dws[0, 0, 0:44, :] = dg_ref[...]
+    bv = bv_ref[...].astype(jnp.float32)
+    dws[0, 0, 44:45, :] = jnp.concatenate([bv[i : i + 1] for i in range(16)], axis=1).astype(jnp.bfloat16)
+    dws[0, 1, 0:44, :] = dup_ref[...]
+    dws[0, 2, 0:44, :] = ddn_ref[...]
+
+    def send(src, dst, s, r, dev):
+        c = pltpu.make_async_remote_copy(
+            src_ref=src, dst_ref=dst, send_sem=s, recv_sem=r, device_id=dev, device_id_type=MESH
+        )
+        c.start()
+        return c
+
+    pl.semaphore_wait(barrier, 64)
+
+    def hop(m, held, axis):
+        then = held + (1 << axis)
+        sem = m * 8 + then
+        return send(dws.at[held, m], dws.at[then, m], s_w.at[sem], r_w.at[sem], beside(axis))
+
+    order = [[(m + i) % 3 for i in range(3)] for m in range(3)]
+    legs = []
+    leg_a = [hop(m, 0, order[m][0]) for m in range(3)]
+    leg_b = [hop(m, 0, order[m][1]) for m in range(3)]
+    legs += [hop(m, 0, order[m][2]) for m in range(3)]
+
+    own = pl.ds(pl.multiple_of(t * width, width), width)
+    xh = hid_ref[...].astype(jnp.float32)
+    nb = (xh * lax.rsqrt(jnp.mean(xh * xh, axis=-1, keepdims=True) + 1e-06) * mixg_ref[...]).astype(jnp.bfloat16)
+    low = jnp.tanh(nt_dot(nb, dd_ref[...])).astype(jnp.bfloat16)
+    pre = dot(low, du_ref[:, own]) + db_ref[:, own]
+    dec = jnp.exp(-jnp.exp(-0.5) * (1.0 / (1.0 + jnp.exp(-pre))))
+    rlow = nt_dot(nb, rd_ref[...]).astype(jnp.bfloat16)
+    lr = 1.0 / (1.0 + jnp.exp(-(dot(rlow, ru_ref[:, own]) + rb_ref[:, own])))
+    for c in aload[:3]:
+        c.wait()
+    key = dot(nb, wk[...]).astype(jnp.bfloat16).astype(jnp.float32)
+    rec = dot(nb, wr[...]).astype(jnp.bfloat16).astype(jnp.float32)
+    val = dot(nb, wv[...]).astype(jnp.bfloat16).astype(jnp.float32)
+    for h in range(heads):
+        cut = slice(h * size, (h + 1) * size)
+        kh, lh, rh, vh = key[:, cut], lr[:, cut], rec[:, cut], val[:, cut]
+        kn = kh * (1.0 / (jnp.sum(kh * kh, axis=-1, keepdims=True) + 1e-06))
+        kl = kh * lh
+        beta = jnp.sum(kl * rh, axis=-1, keepdims=True)
+        k_s[h] = kn
+        d_s[h] = dec[:, cut]
+        l_s[h] = kl
+        v_s[h] = vh
+        g_s[h] = dec[:, cut] * rh - beta * kn
+        bt_s[h] = beta * vh
+
+    for w in leg_a:
         w.wait()
-    legs = leg(1)
+    leg_c = [hop(m, 1 << order[m][0], order[m][1]) for m in range(3)]
+    legs += [hop(m, 1 << order[m][0], order[m][2]) for m in range(3)]
+    for w in leg_b:
+        w.wait()
+    legs += [hop(m, 1 << order[m][1], order[m][2]) for m in range(3)]
 
     lane = iota((size, 128), 1)
     chunks = 64 // CH
@@ -186,10 +188,36 @@
         if c == 3:
             for w in wload:
                 w.start()
-        if c == 5:
-            for w in legs:
-                w.wait()
-            legs = leg(2)
+    eye = iota((size, size), 0) == iota((size, size), 1)
+    again = [
+        pltpu.make_async_copy(st_ref.at[pl.ds(c * CH, CH)], st.at[c % 4], l_again.at[c]) for c in range(4)
+    ]
+    stores = [
+        pltpu.make_async_copy(nsb.at[n % 2], ns_ref.at[pl.ds((n + 4) % 8 * CH, CH)], l_ns.at[n]) for n in range(8)
+    ]
+
+    def update(n):
+        c = (n + 4) % 8
+        if n >= 4:
+            again[c].wait()
+        if n >= 2:
+            stores[n - 2].wait()
+
+        def one(j, _):
+            for u in range(4):
+                sl = j * 4 + u
+                at = pl.ds(c * CH + sl, 1)
+                for h in range(heads):
+                    m = st[c % 4, sl, h]
+                    w = jnp.sum(jnp.where(eye, v_s[h, at, :], 0.0) - m * k_s[h, at, :], axis=-1, keepdims=True)
+                    nsb[n % 2, sl, h] = (m * d_s[h, at, :] + w * l_s[h, at, :]).astype(jnp.bfloat16)
+            return 0
+
+        lax.fori_loop(0, CH // 4, one, 0)
+        stores[n].start()
+        if n < 4:
+            again[n].start()
+
     for h in range(heads):
         y = yt_s[h].T[:64] + bt_s[h]
         cen = y - jnp.mean(y, axis=-1, keepdims=True)
@@ -210,6 +238,20 @@
     ).astype(jnp.bfloat16)
     tok[0, 0:64, :] = ffn[:, :HALF]
     tok[1, 0:64, :] = ffn[:, HALF:]
+    pieces = [(0, 384), (384, 384), (768, 256)]
+
+    def pass_on(m, held, axis):
+        then = held + (1 << axis)
+        cols = pl.ds(*pieces[m])
+        sem = m * 8 + then
+        return send(
+            tok.at[t, pl.ds(held * 64, 64), cols], tok.at[t, pl.ds(then * 64, 64), cols], s_tok.at[sem], r_tok.at[sem],
+            b_peer(1 << axis),
+        )
+
+    tok_a = [pass_on(m, 0, order[m][0]) for m in range(3)]
+    tok_b = [pass_on(m, 0, order[m][1]) for m in range(3)]
+    toks = [pass_on(m, 0, order[m][2]) for m in range(3)]
     for q in range(8):
         tq[q // 4, (q % 4) * 64 : (q % 4 + 1) * 64, :] = ffn[:, q * 256 : (q + 1) * 256]
     disp[...] = dot(pbig[...], tq[t]).astype(jnp.bfloat16).reshape(64, 16, 256)
@@ -221,11 +263,25 @@
 
     lax.fori_loop(1, 64, scatter, 0)
     xin[t, ep] = disp[ep]
-    c_tok = [
-        send(tok.at[t, pl.ds(0, 64), :], tok.at[t, pl.ds(k * 64, 64), :], s_tok.at[k], r_tok.at[k], b_peer(k))
-        for k in range(1, 8)
-    ]
-
+    for n in range(3):
+        update(n)
+    for c in tok_a:
+        c.wait()
+    tok_c = [pass_on(m, 1 << order[m][0], order[m][1]) for m in range(3)]
+    toks += [pass_on(m, 1 << order[m][0], order[m][2]) for m in range(3)]
+    for c in tok_b:
+        c.wait()
+    toks += [pass_on(m, 1 << order[m][1], order[m][2]) for m in range(3)]
+    for n in range(3, 6):
+        update(n)
+    for c in tok_c:
+        c.wait()
+    toks += [pass_on(m, (1 << order[m][0]) + (1 << order[m][1]), order[m][2]) for m in range(3)]
+    for w in leg_c:
+        w.wait()
+    legs += [hop(m, (1 << order[m][0]) + (1 << order[m][1]), order[m][2]) for m in range(3)]
+    for n in range(6, 8):
+        update(n)
     most = pl.ds(0, 63)
     c_dis = pltpu.make_async_remote_copy(
         src_ref=disp.at[most], dst_ref=xin.at[t, most], send_sem=s_dis, recv_sem=r_dis, device_id=mate,
@@ -251,37 +307,22 @@
     g = dot(xs[0], wg[:HALF]) + dot(xs[1], wg[HALF:])
     u = dot(xs[0], wu[:HALF]) + dot(xs[1], wu[HALF:])
     act = (g / (1.0 + jnp.exp(-g)) * u).astype(jnp.bfloat16)
+    for c in toks:
+        c.wait()
+    others = pl.ds(64, 448)
+    c_fwd = send(tok.at[t, others, :], tok.at[t, others, :], s_fwd, r_fwd, mate)
     ybuf[0] = dot(act, wdn[:, :HALF])
     ybuf[1] = dot(act, wdn[:, HALF:])
     ysend[...] = ybuf[1 - t].astype(jnp.bfloat16)
     c_y = send(ysend, yrecv, s_y, r_y, mate)
-    c_fwd = []
-    for k in range(1, 8):
-        c_tok[k - 1].wait()
-        his = pl.ds(k * 64, 64)
-        c_fwd.append(send(tok.at[t, his, :], tok.at[t, his, :], s_fwd.at[k], r_fwd.at[k], mate))
-
-    c_y.wait()
-    z = (ybuf[t] + yrecv[...].astype(jnp.float32)).astype(jnp.bfloat16)
-    for m in range(4):
-        block = jnp.concatenate([z[m * 64 : (m + 1) * 64, q * 256 : (q + 1) * 256] for q in range(4)], axis=0)
-        zsend[m * 16 : (m + 1) * 16] = dot(ungroup, block).astype(jnp.bfloat16).reshape(16, 16, 256)
-
-    def gather(k, _):
-        e = (ep + k) % 64
-        send(zsend.at[e], ret.at[ep], s_ret, r_ret, (e, t))
-        return 0
-
-    lax.fori_loop(1, 64, gather, 0)
-    ret[ep] = zsend[ep]
-
-    for c in legs + c_fwd:
-        c.wait()
+    for c in legs:
+        c.wait()
+    c_fwd.wait()
     gate = dws[:, 0].reshape(384, 2048)
     up = dws[:, 1].reshape(384, 2048)
     down = dws[:, 2].reshape(384, 2048)
-    c_dn = []
-    for p in range(2):
+
+    def dense(p):
         part_rows = slice(p * 256, p * 256 + 256)
         t0, t1 = tok[0, part_rows, :], tok[1, part_rows, :]
         g = nt_dot(t0, gate[:, :HALF]) + nt_dot(t1, gate[:, HALF:])
@@ -291,16 +332,57 @@
         dbuf[p, 0] = dot(act, down[:, :HALF]) * blend
         dbuf[p, 1] = dot(act, down[:, HALF:]) * blend
         dsend[p] = dbuf[p, 1 - t].astype(jnp.bfloat16)
-        c_dn.append(send(dsend.at[p], drecv.at[p], s_dn.at[p], r_dn.at[p], mate))
-    c_rs = []
-    for p in range(2):
-        c_dn[p].wait()
+        return send(dsend.at[p], drecv.at[p], s_dn.at[p], r_dn.at[p], mate)
+
+    def homeward(p):
         rsend[p * 4 : p * 4 + 4] = (
             (dbuf[p, t] + drecv[p].astype(jnp.float32)).astype(jnp.bfloat16).reshape(4, 64, HALF)
         )
-        for k in range(p * 4, p * 4 + 4):
-            if k:
-                c_rs.append(send(rsend.at[k], rs.at[k], s_rs.at[k], r_rs.at[k], b_peer(k)))
+
+    c_dn = dense(0)
+    c_y.wait()
+    z = (ybuf[t] + yrecv[...].astype(jnp.float32)).astype(jnp.bfloat16)
+    for m in range(4):
+        block = jnp.concatenate([z[m * 64 : (m + 1) * 64, q * 256 : (q + 1) * 256] for q in range(4)], axis=0)
+        zsend[m * 16 : (m + 1) * 16] = dot(ungroup, block).astype(jnp.bfloat16).reshape(16, 16, 256)
+
+    def gather(k, _):
+        e = (ep + k) % 64
+        send(zsend.at[e], ret.at[ep], s_ret, r_ret, (e, t))
+        return 0
+
+    lax.fori_loop(1, 64, gather, 0)
+    ret[ep] = zsend[ep]
+
+    c_dn.wait()
+    homeward(0)
+    c_dn = dense(1)
+    c_dn.wait()
+    homeward(1)
+    c_rs = []
+    for m in range(3):
+        cols, axis = pl.ds(*pieces[m]), order[m][0]
+        for k in range(8):
+            if k >> axis & 1:
+                c_rs.append(send(
+                    rsend.at[k, :, cols], rs.at[k - (1 << axis), :, cols], s_rs.at[m * 8 + k], r_rs.at[m * 8 + k],
+                    b_peer(1 << axis),
+                ))
+    for c in c_rs:
+        c.wait()
+    c_rs, totals = [], []
+    for m in range(3):
+        cols, axis = slice(pieces[m][0], sum(pieces[m])), order[m][0]
+        for k in range(8):
+            if not k >> axis & 1:
+                both = rsend[k, :, cols].astype(jnp.float32) + rs[k, :, cols].astype(jnp.float32)
+                if k:
+                    rsend[k, :, cols] = both.astype(jnp.bfloat16)
+                    c_rs.append(send(
+                        rsend.at[k, :, cols], rs2.at[k, :, cols], s_rs.at[m * 8 + k], r_rs.at[m * 8 + k], b_peer(k)
+                    ))
+                else:
+                    totals.append(both)
 
     c_ret = pltpu.make_async_remote_copy(
         src_ref=zsend.at[most], dst_ref=ret.at[most], send_sem=s_ret, recv_sem=r_ret, device_id=mate,
@@ -310,14 +392,19 @@
     comb = dot(pst[...], ret[...].reshape(1024, 256))
     for c in c_rs:
         c.wait()
-    total = fres[t].astype(jnp.float32) + rsend[0].astype(jnp.float32)
-    for i in range(1, 8):
-        total += rs[i].astype(jnp.float32)
+    for m in range(3):
+        cols, axis = slice(pieces[m][0], sum(pieces[m])), order[m][0]
+        for k in range(1, 8):
+            if not k >> axis & 1:
+                totals[m] += rs2[k, :, cols].astype(jnp.float32)
+    total = fres[t].astype(jnp.float32) + jnp.concatenate(totals, axis=1)
     for q in range(4):
         piece = slice(q * 256, (q + 1) * 256)
         obuf[t, :, piece] = (total[:, piece] + comb[q * 64 : (q + 1) * 64]).astype(jnp.bfloat16)
     c_out = send(obuf.at[t], obuf.at[t], s_out, r_out, mate)
     c_out.wait()
+    stores[6].wait()
+    stores[7].wait()
     out_ref[:, :HALF] = obuf[0]
     out_ref[:, HALF:] = obuf[1]
 
@@ -328,7 +415,7 @@
     bf, f4 = jnp.bfloat16, jnp.float32
     dma = pltpu.SemaphoreType.DMA
     v = pltpu.VMEM
-    scratch = [v(ref.shape, bf) for ref in large[:8]] + [
+    scratch = [v((4, 8, 64, 64), f4), v((2, CH, 8, 64, 64), bf)] + [v(ref.shape, bf) for ref in large[:8]] + [
         v((2048, 512), bf), v((2048, 512), bf), v((2048, 512), bf), v((512, 2048), bf),
         v((4, CH, 8, 64, 64), f4),
         v((8, 64, 64), f4), v((8, 64, 64), f4), v((8, 64, 128), f4),
@@ -340,15 +427,15 @@
         v((2, 256, HALF), f4), v((256, HALF), bf), v((256, HALF), bf),
         v((64, 16, 256), bf), v((64, 16, 256), bf),
         v((2, 2, 256, HALF), f4), v((2, 256, HALF), bf), v((2, 256, HALF), bf),
-        v((8, 64, HALF), bf), v((8, 64, HALF), bf), v((2, 64, HALF), bf),
-        dma((8,)), dma((4,)), dma((8,)), dma((3,)), dma, dma, dma((8,)), dma((8,)), dma((8,)), dma((8,)), dma, dma, dma,
-        dma, dma, dma, dma, dma, dma((2,)), dma((2,)), dma((8,)), dma((8,)), dma, dma, dma((24,)), dma((24,)),
+        v((8, 64, HALF), bf), v((8, 64, HALF), bf), v((8, 64, HALF), bf), v((2, 64, HALF), bf),
+        dma((8,)), dma((4,)), dma((8,)), dma((4,)), dma((8,)), dma((3,)), dma, dma, dma((24,)), dma((24,)), dma, dma, dma, dma, dma,
+        dma, dma, dma, dma, dma, dma((2,)), dma((2,)), dma((24,)), dma((24,)), dma, dma, dma((24,)), dma((24,)),
     ]
     return pl.pallas_call(
         layer_kernel,
-        out_shape=[jax.ShapeDtypeStruct((64, 2048), bf), jax.ShapeDtypeStruct((4, 8, 64, 64), f4)],
+        out_shape=[jax.ShapeDtypeStruct((64, 2048), bf), jax.ShapeDtypeStruct((64, 8, 64, 64), bf)],
         in_specs=[vm] * len(small) + [anyw] * len(large),
-        out_specs=[vm] * 2,
+        out_specs=[vm, anyw],
         scratch_shapes=scratch,
         compiler_params=pltpu.CompilerParams(
             collective_id=0, has_side_effects=True, vmem_limit_bytes=63 * 1024 * 1024
@@ -360,7 +447,7 @@
 SB = 4
 
 
-def state_kernel(rows_ref, tokens_ref, st_ref, ns_ref, out_ref, old, new, l_in, l_out):
+def state_kernel(tokens_in, st_ref, ns_ref, out_ref, old, new, l_t, l_in, l_out):
     count = st_ref.shape[0] // SB
 
     def load(c):
@@ -373,24 +460,19 @@
 
     for c in range(count):
         load(c).start()
-    out_ref[...] = tokens_ref[...]
-    eye = iota((64, 64), 0) == iota((64, 64), 1)
+    tokens = pltpu.make_async_copy(tokens_in, out_ref, l_t)
+    tokens.start()
 
     def one(c, _):
         load(c).wait()
         for u in range(SB):
-            s = c * SB + u
-            row = pl.ds(s, 1)
             for h in range(8):
-                m = old[s, h]
-                w = jnp.sum(
-                    jnp.where(eye, rows_ref[3, h, row, :], 0.0) - m * rows_ref[0, h, row, :], axis=-1, keepdims=True
-                )
-                new[s, h] = m * rows_ref[1, h, row, :] + w * rows_ref[2, h, row, :]
+                new[c * SB + u, h] = old[c * SB + u, h].astype(jnp.float32)
         store(c).start()
         return 0
 
     lax.fori_loop(0, count, one, 0)
+    tokens.wait()
 
     def drain(c, _):
         store(c).wait()
@@ -399,26 +481,27 @@
     lax.fori_loop(0, count, drain, 0)
 
 
-def new_states(rows, tokens, state):
+def wide_states(tokens, state):
     vm = pl.BlockSpec(memory_space=pltpu.VMEM)
     anyw = pl.BlockSpec(memory_space=pl.ANY)
     return pl.pallas_call(
         state_kernel,
-        in_specs=[vm, vm, anyw],
+        in_specs=[anyw, anyw],
         out_specs=[anyw, vm],
         out_shape=[
             jax.ShapeDtypeStruct(state.shape, jnp.float32),
             jax.ShapeDtypeStruct(tokens.shape, jnp.bfloat16),
         ],
         scratch_shapes=[
+            pltpu.VMEM(state.shape, jnp.bfloat16),
             pltpu.VMEM(state.shape, jnp.float32),
-            pltpu.VMEM(state.shape, jnp.float32),
+            pltpu.SemaphoreType.DMA,
             pltpu.SemaphoreType.DMA((state.shape[0] // SB,)),
             pltpu.SemaphoreType.DMA((state.shape[0] // SB,)),
         ],
         compiler_params=pltpu.CompilerParams(vmem_limit_bytes=63 * 1024 * 1024),
         name="states",
-    )(rows, tokens, state)
+    )(tokens, state)
 
 
 def shards(
@@ -435,8 +518,8 @@
         hidden, decay_down.T, decay_up, rate_down.T, rate_up, dense_gate.T, dense_up.T, dense_down,
         recept_weight, key_weight, value_weight, out_weight, memory_state, expert_gate, expert_up, expert_down,
     ]
-    tokens, rows = layer(small, large)
-    new_state, layer_out = new_states(rows, tokens, memory_state)
+    tokens, states = layer(small, large)
+    new_state, layer_out = wide_states(tokens, states)
     return (layer_out, new_state)
 
 

time: 94.2 us -> 84.7 us (0.90)
  Pallas kernels: 93.2 us -> 83.7 us
    pallas_call x1, Pallas kernels: 13.9 us -> 9.03 us  [wide_states(): pl.pallas_call(state_kernel, in_specs=[anyw, anyw], out_specs=[anyw, vm],...]
    pallas_call x1, Pallas kernels: 79.2 us -> 74.7 us  [layer(): pl.pallas_call(layer_kernel, out_shape=[jax.ShapeDtypeStruct((64, 2048),...]
where the time goes in v5:
time: 84.7 us; the launch traced here: 84.5 us
  Pallas kernels  83.7 us (99%)
    pallas_call x1, Pallas kernels, layer(): pl.pallas_call(layer_kernel, out_shape=[jax.ShapeDtypeStruct((64, 2048),...  74.7 us
    pallas_call x1, Pallas kernels, wide_states(): pl.pallas_call(state_kernel, in_specs=[anyw, anyw], out_specs=[anyw, vm],...  9.03 us

profile of v5, /device:TPU:1, one launch (start us, length us, event | category | flops | bytes accessed | tf_op | source)
XLA Modules:
  0.0 84.5 jit_solution(2806043689544044098)
XLA Ops:
  0.6 74.7 %layer.1 = (bf16[64,2048]{1,0:T(8,128)(2,1)}, bf16[64,8,64,64]{3,2,1,0:T(8,128)(2,1)}) custom-call(f32[1,2048]{1,0:T(1,128)} %bitcast.16, f32[1,1024]{1,0:T(1,128)} %bitcast.18, f32[1,1024]{1,0:T(1,128)} %bitcast.19, f32[1,1024]{1,0:T(1,128)} %bitcast.20, f32[1,2048]{1,0:T(1,128)} %bitcast.17, bf16[16,128]{1,0:T(8,128)(2,1)} %bitcast.21, s32[2,64]{1,0:T(2,128)} %bitcast.22, ...), custom_call_target="tpu_custom_call" | custom-call | tf_op jit(solution)/shard_map/layer/pallas_call | solution.py:434
  75.3 9.0 %states.1 = (f32[64,8,64,64]{3,2,1,0:T(8,128)}, bf16[64,2048]{1,0:T(8,128)(2,1)}) custom-call(bf16[64,2048]{1,0:T(8,128)(2,1)} %get-tuple-element.6.tokens_in, bf16[64,8,64,64]{3,2,1,0:T(8,128)(2,1)} %get-tuple-element.7.st_ref), custom_call_target="tpu_custom_call" | custom-call | tf_op jit(solution)/shard_map/states/pallas_call | solution.py:487

commit v6 on v5

--- a/solution.py
+++ b/solution.py
@@ -71,7 +71,7 @@
         pl.semaphore_signal(barrier, inc=1, device_id=((ep + k) % 64, t), device_id_type=MESH)
         return 0
 
-    lax.fori_loop(1, 64, greet, 0)
+    lax.fori_loop(1, 64, greet, 0, unroll=7)
 
     aload = [
         pltpu.make_async_copy(src, dst, l_a.at[i])
@@ -261,7 +261,7 @@
         send(disp.at[e], xin.at[t, ep], s_dis, r_dis, (e, t))
         return 0
 
-    lax.fori_loop(1, 64, scatter, 0)
+    lax.fori_loop(1, 64, scatter, 0, unroll=7)
     xin[t, ep] = disp[ep]
     for n in range(3):
         update(n)
@@ -351,7 +351,7 @@
         send(zsend.at[e], ret.at[ep], s_ret, r_ret, (e, t))
         return 0
 
-    lax.fori_loop(1, 64, gather, 0)
+    lax.fori_loop(1, 64, gather, 0, unroll=7)
     ret[ep] = zsend[ep]
 
     c_dn.wait()

time: 84.7 us -> 84.7 us (level)
  no operation moved by 1% of the time
where the time goes in v6:
time: 84.7 us; the launch traced here: 84.6 us
  Pallas kernels  83.8 us (99%)
    pallas_call x1, Pallas kernels, layer(): pl.pallas_call(layer_kernel, out_shape=[jax.ShapeDtypeStruct((64, 2048),...  74.8 us
    pallas_call x1, Pallas kernels, wide_states(): pl.pallas_call(state_kernel, in_specs=[anyw, anyw], out_specs=[anyw, vm],...  9.03 us

profile of v6, /device:TPU:1, one launch (start us, length us, event | category | flops | bytes accessed | tf_op | source)
XLA Modules:
  0.0 84.6 jit_solution(15606110139511305418)
XLA Ops:
  0.6 74.8 %layer.1 = (bf16[64,2048]{1,0:T(8,128)(2,1)}, bf16[64,8,64,64]{3,2,1,0:T(8,128)(2,1)}) custom-call(f32[1,2048]{1,0:T(1,128)} %bitcast.16, f32[1,1024]{1,0:T(1,128)} %bitcast.18, f32[1,1024]{1,0:T(1,128)} %bitcast.19, f32[1,1024]{1,0:T(1,128)} %bitcast.20, f32[1,2048]{1,0:T(1,128)} %bitcast.17, bf16[16,128]{1,0:T(8,128)(2,1)} %bitcast.21, s32[2,64]{1,0:T(2,128)} %bitcast.22, ...), custom_call_target="tpu_custom_call" | custom-call | tf_op jit(solution)/shard_map/layer/pallas_call | solution.py:434
  75.4 9.0 %states.1 = (f32[64,8,64,64]{3,2,1,0:T(8,128)}, bf16[64,2048]{1,0:T(8,128)(2,1)}) custom-call(bf16[64,2048]{1,0:T(8,128)(2,1)} %get-tuple-element.6.tokens_in, bf16[64,8,64,64]{3,2,1,0:T(8,128)(2,1)} %get-tuple-element.7.st_ref), custom_call_target="tpu_custom_call" | custom-call | tf_op jit(solution)/shard_map/states/pallas_call | solution.py:487
